TPU v7x, 128 devices: a whole 4x4x4 slice. The times are simulated.
128 devices in a mesh: tp: 16 (over z, y), dp: 8 (over x, core).
Axes of the slice: x: 4, y: 4, z: 4, core: 2. Of those that a mesh axis runs over, the one named last changes fastest.
Arguments:
- tokens: bfloat16 [256, 4096], P('dp', 'tp'), may hold values from -6 to 6
- lengths: int32 [256], P('dp'), may hold values from 1 to 96, 6144 in all
- norm_gain: float32 [2, 4096], replicated, may hold values from 0.1 to 1.9
- w_recept: bfloat16 [2, 4096, 4096], P(None, None, ('tp', 'dp')), may hold values from -0.09375 to 0.09375
- w_key: bfloat16 [2, 4096, 4096], P(None, None, ('tp', 'dp')), may hold values from -0.09375 to 0.09375
- w_value: bfloat16 [2, 4096, 4096], P(None, None, ('tp', 'dp')), may hold values from -0.09375 to 0.09375
- w_decay: bfloat16 [2, 4096, 4096], P(None, None, ('tp', 'dp')), may hold values from -0.09375 to 0.09375
- w_rate: bfloat16 [2, 4096, 4096], P(None, None, ('tp', 'dp')), may hold values from -0.09375 to 0.09375
- w_gate: bfloat16 [2, 4096, 4096], P(None, None, ('tp', 'dp')), may hold values from -0.09375 to 0.09375
- w_out: bfloat16 [2, 4096, 4096], P(None, None, ('tp', 'dp')), may hold values from -0.09375 to 0.09375
- decay_base: float32 [2, 4096], P(None, 'tp'), may hold values from -3 to 1
- rate_base: float32 [2, 4096], P(None, 'tp'), may hold values from -3 to 3
- group_gain: float32 [2, 4096], P(None, 'tp'), may hold values from 0.1 to 1.9
- state: float32 [2, 256, 64, 64, 64], P(None, 'dp', 'tp'), may hold values from -6 to 6
Outputs:
- mixed: bfloat16 [256, 4096], P('dp', 'tp')
- new_state: float32 [2, 256, 64, 64, 64], P(None, 'dp', 'tp')
Inputs may be any that keep to these rules, and one draw needn't show every extreme that they name: Each sequence's live length lies between 1 and 96, some sequences reach 96, and the lengths sum to 6144.
All inputs are finite; a program needn't handle non-finite values.
Results may differ from a plain program's by a relative error of at most 0.025.
Values may be sent and summed in bfloat16 or wider, within the bound.
A program may use at most 128 MiB of HBM per device.

v0:
```python
import jax
import jax.numpy as jnp
from jax import lax
from jax.sharding import Mesh
from jax.sharding import PartitionSpec as P

STEP = 16
TP = ("tp_0", "tp_1")
TP_DP = ("tp_0", "tp_1", "dp")


RMS_EPS = 1e-06
GROUP_EPS = 0.00064


def gather_axes(value, axes, dim):
    if not axes:
        return value
    nearer = lax.all_gather(value, axes[-1], axis=dim, tiled=True)
    return gather_axes(nearer, axes[:-1], dim)


def shortened(value):
    def short(part):
        return part.astype(jnp.bfloat16) if part.dtype == jnp.float32 else part

    return jax.tree.map(short, value)


def over_axes(value, axes, dim, absorb, carry):
    everything = jax.tree.map(lambda part: gather_axes(part, axes, dim), value)
    return absorb(carry, everything, jnp.int32(0))


def recur(state_old, recept, key_vec, value_vec, decay_rate, learn_rate, active, head_size):
    split = (recept.shape[0], -1, head_size)
    recept_h = recept.reshape(split)
    key_h = key_vec.reshape(split)
    value_h = value_vec.reshape(split)
    decay_h = decay_rate.reshape(split)
    rate_h = learn_rate.reshape(split)
    key_len = jnp.sqrt(jnp.sum(key_h * key_h, axis=-1, keepdims=True))
    key_unit = key_h / jnp.maximum(key_len, 1e-12)
    state_a = jnp.einsum("bhij,bhj->bhi", state_old, -key_unit, precision=lax.Precision.DEFAULT)
    updated = (
        state_old * decay_h[:, :, None, :]
        + state_a[:, :, :, None] * (key_unit * rate_h)[:, :, None, :]
        + value_h[:, :, :, None] * (key_h * rate_h)[:, :, None, :]
    )
    updated = jnp.where(active[:, None, None, None], updated, state_old)
    readout = jnp.einsum("bhij,bhj->bhi", updated, recept_h, precision=lax.Precision.DEFAULT)
    centre = jnp.mean(readout, axis=-1, keepdims=True)
    spread = jnp.mean(jnp.square(readout - centre), axis=-1, keepdims=True)
    normal_out = ((readout - centre) * lax.rsqrt(spread + GROUP_EPS)).reshape(recept.shape[0], -1)
    return (updated, normal_out)


def local(
    tokens,
    lengths,
    norm_gain,
    w_recept,
    w_key,
    w_value,
    w_decay,
    w_rate,
    w_gate,
    w_out,
    decay_base,
    rate_base,
    group_gain,
    state,
):
    slim = w_recept.shape[2]
    head_size = state.shape[-1]
    active = lengths > STEP
    current = tokens
    updated_states = []
    for layer_idx in range(2):
        joined = jnp.concatenate(
            [
                w_recept[layer_idx],
                w_key[layer_idx],
                w_value[layer_idx],
                w_decay[layer_idx],
                w_rate[layer_idx],
                w_gate[layer_idx],
            ],
            axis=1,
        )
        batch_raw = lax.all_gather(current, "dp", axis=0, tiled=True)
        every_feature = gather_axes(batch_raw, TP, 1)
        values = every_feature.astype(jnp.float32)
        factor = lax.rsqrt(jnp.mean(values * values, axis=1, keepdims=True) + RMS_EPS)
        normed = (values * factor * norm_gain[layer_idx]).astype(jnp.bfloat16)
        projected = jnp.dot(normed, joined, preferred_element_type=jnp.float32)
        pieces = [
            projected[:, idx * slim : (idx + 1) * slim].astype(jnp.bfloat16) for idx in range(6)
        ]
        arrived = (
            lax.all_to_all(shortened(pieces[0]), "dp", split_axis=0, concat_axis=1, tiled=True),
            lax.all_to_all(shortened(pieces[1]), "dp", split_axis=0, concat_axis=1, tiled=True),
            lax.all_to_all(shortened(pieces[2]), "dp", split_axis=0, concat_axis=1, tiled=True),
            lax.all_to_all(shortened(pieces[3]), "dp", split_axis=0, concat_axis=1, tiled=True),
            lax.all_to_all(shortened(pieces[4]), "dp", split_axis=0, concat_axis=1, tiled=True),
            lax.all_to_all(shortened(pieces[5]), "dp", split_axis=0, concat_axis=1, tiled=True),
        )
        recept, key_vec, value_vec, decay_pre, rate_pre, gate_pre = [
            item.astype(jnp.float32) for item in arrived
        ]
        decay_rate = jnp.exp(-jnp.exp(-jax.nn.softplus(-(decay_base[layer_idx] + decay_pre)) - 0.5))
        learn_rate = jax.nn.sigmoid(rate_base[layer_idx] + rate_pre)
        gate_open = jax.nn.sigmoid(gate_pre)
        updated, normal_out = recur(
            state[layer_idx], recept, key_vec, value_vec, decay_rate, learn_rate, active, head_size
        )
        updated_states.append(updated)
        mixed_here = jnp.where(
            active[:, None], normal_out * group_gain[layer_idx] * gate_open, 0.0
        ).astype(jnp.bfloat16)
        rows_all = lax.all_gather(mixed_here, "dp", axis=0, tiled=True)
        out_weight = w_out[layer_idx]

        def fold_output(acc_sum, segment, offset):
            weight_rows = lax.dynamic_slice_in_dim(out_weight, offset, segment.shape[1], 0)
            return acc_sum + jnp.dot(segment, weight_rows, preferred_element_type=jnp.float32)

        blank = jnp.zeros((rows_all.shape[0], out_weight.shape[1]), jnp.float32)
        out_cols = over_axes(rows_all, TP, 1, fold_output, blank).astype(jnp.bfloat16)
        current = lax.all_to_all(out_cols, "dp", split_axis=0, concat_axis=1, tiled=True)
    return (current, jnp.stack(updated_states))


def solution(mesh):
    finer = Mesh(mesh.devices.reshape(4, 4, mesh.shape["dp"]), ("tp_0", "tp_1", "dp"))
    in_specs = (
        P("dp", TP),
        P("dp"),
        P(),
        P(None, None, TP_DP),
        P(None, None, TP_DP),
        P(None, None, TP_DP),
        P(None, None, TP_DP),
        P(None, None, TP_DP),
        P(None, None, TP_DP),
        P(None, None, TP_DP),
        P(None, TP),
        P(None, TP),
        P(None, TP),
        P(None, "dp", TP, None, None),
    )
    out_specs = (P("dp", TP), P(None, "dp", TP, None, None))
    return jax.shard_map(local, mesh=finer, in_specs=in_specs, out_specs=out_specs, check_vma=False)
```

profile of v0, /device:TPU:0, one launch (start us, length us, event | category | flops | bytes accessed | tf_op | source)
XLA Modules:
  0.0 406.6 jit_solution(4203968245207242246)
XLA Ops:
  7.3 13.6 %all_gather.36 = bf16[256,256]{1,0:T(8,128)(2,1)S(1)} all-gather(bf16[32,256]{1,0:T(8,128)(2,1)} %param.14), channel_id=1, replica_groups=mesh['tp_0'=4,'tp_1'=4,'dp'=8] {'dp'}, dimensions={0}, use_global_device_ids=true | all-gather | bytes 147456 | tf_op jit(solution)/shard_map/all_gather | solution.py:91
  20.9 14.1 %all_gather.37 = bf16[256,1024]{1,0:T(8,128)(2,1)} all-gather(bf16[256,256]{1,0:T(8,128)(2,1)S(1)} %all_gather.36), channel_id=1, replica_groups=mesh['tp_0'=4,'tp_1'=4,'dp'=8] {'tp_1'}, dimensions={1}, use_global_device_ids=true | all-gather | bytes 655360 | tf_op jit(solution)/shard_map/all_gather | solution.py:19
  35.0 0.9 fusion.74
  35.9 1.8 bitcast_dynamic-update-slice_fusion.11
  37.6 1.8 bitcast_dynamic-update-slice_fusion.10
  39.4 1.8 bitcast_dynamic-update-slice_fusion.9
  41.2 0.7 bitcast_dynamic-update-slice_fusion.8
  41.9 0.7 bitcast_dynamic-update-slice_fusion.7
  42.7 0.7 bitcast_dynamic-update-slice_fusion.6
  43.4 24.0 %all-gather.5.cloned.1.call-done = bf16[256,4096]{1,0:T(8,128)(2,1)} async-done(((bf16[256,1024]{1,0:T(8,128)(2,1)}), bf16[256,4096]{1,0:T(8,128)(2,1)}) %all-gather.5.cloned.1.call-update) | async-done | bytes 2097168 | tf_op jit(solution)/shard_map/all_gather | solution.py:19
  67.5 2.1 fusion
  69.6 2.5 fusion.44
  72.9 4.3 %all-to-all-start = ((bf16[8,2,512]{2,1,0:T(2,128)(2,1)}), bf16[8,2,512]{2,1,0:T(2,128)(2,1)S(1)}, u32[]{:S(2)}, u32[]{:S(2)}) async-start(bf16[8,2,512]{2,1,0:T(2,128)(2,1)} %reshape.354), calls=%async_computation | async-start | bytes 32768 | tf_op jit(solution)/shard_map/all_to_all | solution.py:104
  77.5 0.7 reshape.344
  78.4 0.7 reshape.346
  79.2 0.7 reshape.352
  81.6 0.9 all-to-all-done
  82.6 3.9 all-to-all-start.5
  86.5 5.2 %all-to-all-done.5 = bf16[8,2,512]{2,1,0:T(2,128)(2,1)S(1)} async-done(((bf16[8,2,512]{2,1,0:T(2,128)(2,1)}), bf16[8,2,512]{2,1,0:T(2,128)(2,1)S(1)}, u32[]{:S(2)}, u32[]{:S(2)}) %all-to-all-start.5) | async-done | bytes 16416 | tf_op jit(solution)/shard_map/all_to_all | solution.py:106
  91.8 3.3 all-to-all-start.3
  95.2 5.1 %all-to-all-done.3 = bf16[8,2,512]{2,1,0:T(2,128)(2,1)S(1)} async-done(((bf16[8,2,512]{2,1,0:T(2,128)(2,1)}), bf16[8,2,512]{2,1,0:T(2,128)(2,1)S(1)}, u32[]{:S(2)}, u32[]{:S(2)}) %all-to-all-start.3) | async-done | bytes 16416 | tf_op jit(solution)/shard_map/all_to_all | solution.py:103
  100.4 3.3 all-to-all-start.1
  103.8 5.2 %all-to-all-done.1 = bf16[8,2,512]{2,1,0:T(2,128)(2,1)S(1)} async-done(((bf16[8,2,512]{2,1,0:T(2,128)(2,1)}), bf16[8,2,512]{2,1,0:T(2,128)(2,1)S(1)}, u32[]{:S(2)}, u32[]{:S(2)}) %all-to-all-start.1) | async-done | bytes 16416 | tf_op jit(solution)/shard_map/all_to_all | solution.py:102
  109.0 3.3 all-to-all-start.4
  112.4 5.2 %all-to-all-done.4 = bf16[8,2,512]{2,1,0:T(2,128)(2,1)S(1)} async-done(((bf16[8,2,512]{2,1,0:T(2,128)(2,1)}), bf16[8,2,512]{2,1,0:T(2,128)(2,1)S(1)}, u32[]{:S(2)}, u32[]{:S(2)}) %all-to-all-start.4) | async-done | bytes 16416 | tf_op jit(solution)/shard_map/all_to_all | solution.py:101
  117.6 3.3 all-to-all-start.2
  121.9 4.3 %all-to-all-done.2 = bf16[8,2,512]{2,1,0:T(2,128)(2,1)S(1)} async-done(((bf16[8,2,512]{2,1,0:T(2,128)(2,1)}), bf16[8,2,512]{2,1,0:T(2,128)(2,1)S(1)}, u32[]{:S(2)}, u32[]{:S(2)}) %all-to-all-start.2) | async-done | bytes 16416 | tf_op jit(solution)/shard_map/all_to_all | solution.py:105
  127.1 3.4 fusion.6
  130.4 4.2 %fusion.10 = f32[32,4,1,64]{3,2,1,0:T(1,128)S(1)} fusion(bf16[32,4,64,1]{2,3,1,0:T(2,128)(2,1)S(1)} %reshape.319, f32[2,32,4,64,64]{4,3,2,1,0:T(8,128)} %param.27, f32[32,4,64]{2,1,0:T(4,128)S(1)} %get-tuple-element.29, f32[32,4,64]{2,1,0:T(4,128)S(1)} %reshape.301, f32[32,4,64]{2,1,0:T(4,128)S(1)} %get-tuple-element.28, f32[32,4,64]{2,1,0:T(4,128)S(1)} %bitcast.139, ...), kind=kOutput, calls=%fused_computation.17 | convolution fusion | flops 4194304 | bytes 4407328 | tf_op jit(solution)/shard_map/bhij,bhj->bhi/dot_general | solution.py:51
  135.3 12.7 %all_gather.39 = bf16[256,256]{1,0:T(8,128)(2,1)S(1)} all-gather(bf16[32,256]{1,0:T(8,128)(2,1)S(1)} %select_convert_fusion.1), channel_id=1, replica_groups=mesh['tp_0'=4,'tp_1'=4,'dp'=8] {'dp'}, dimensions={0}, use_global_device_ids=true | all-gather | bytes 147456 | tf_op jit(solution)/shard_map/all_gather | solution.py:121
  148.1 13.9 %all_gather.40 = bf16[256,1024]{1,0:T(8,128)(2,1)} all-gather(bf16[256,256]{1,0:T(8,128)(2,1)S(1)} %all_gather.39), channel_id=1, replica_groups=mesh['tp_0'=4,'tp_1'=4,'dp'=8] {'tp_1'}, dimensions={1}, use_global_device_ids=true | all-gather | bytes 655360 | tf_op jit(solution)/shard_map/all_gather | solution.py:19
  162.1 29.0 %all-gather.7.cloned.1.call-done = bf16[256,4096]{1,0:T(8,128)(2,1)} async-done(((bf16[256,1024]{1,0:T(8,128)(2,1)}), bf16[256,4096]{1,0:T(8,128)(2,1)}) %all-gather.7.cloned.1.call-update) | async-done | bytes 2097168 | tf_op jit(solution)/shard_map/all_gather | solution.py:19
  191.1 2.3 convolution_convert_fusion.1
  193.6 9.4 %all_to_all.200 = bf16[8,2,512]{2,1,0:T(2,128)(2,1)S(1)} all-to-all(bf16[8,2,512]{2,1,0:T(2,128)(2,1)S(1)} %reshape.356), channel_id=1, replica_groups=mesh['tp_0'=4,'tp_1'=4,'dp'=8] {'dp'}, dimensions={0} | all-to-all | bytes 32768 | tf_op jit(solution)/shard_map/all_to_all | solution.py:130
  203.3 12.8 %all_gather.42 = bf16[256,256]{1,0:T(8,128)(2,1)S(1)} all-gather(bf16[32,256]{1,0:T(8,128)(2,1)S(1)} %all_to_all.168), channel_id=1, replica_groups=mesh['tp_0'=4,'tp_1'=4,'dp'=8] {'dp'}, dimensions={0}, use_global_device_ids=true | all-gather | bytes 147456 | tf_op jit(solution)/shard_map/all_gather | solution.py:91
  216.1 13.9 %all_gather.43 = bf16[256,1024]{1,0:T(8,128)(2,1)} all-gather(bf16[256,256]{1,0:T(8,128)(2,1)S(1)} %all_gather.42), channel_id=1, replica_groups=mesh['tp_0'=4,'tp_1'=4,'dp'=8] {'tp_1'}, dimensions={1}, use_global_device_ids=true | all-gather | bytes 655360 | tf_op jit(solution)/shard_map/all_gather | solution.py:19
  230.0 29.1 %all-gather.9.cloned.1.call-done = bf16[256,4096]{1,0:T(8,128)(2,1)} async-done(((bf16[256,1024]{1,0:T(8,128)(2,1)}), bf16[256,4096]{1,0:T(8,128)(2,1)}) %all-gather.9.cloned.1.call-update) | async-done | bytes 2097168 | tf_op jit(solution)/shard_map/all_gather | solution.py:19
  259.1 2.1 fusion.3
  261.2 3.0 fusion.47
  265.0 4.3 %all-to-all-start.7 = ((bf16[8,2,512]{2,1,0:T(2,128)(2,1)}), bf16[8,2,512]{2,1,0:T(2,128)(2,1)S(1)}, u32[]{:S(2)}, u32[]{:S(2)}) async-start(bf16[8,2,512]{2,1,0:T(2,128)(2,1)} %reshape.368), calls=%async_computation.7 | async-start | bytes 32768 | tf_op jit(solution)/shard_map/all_to_all | solution.py:104
  269.5 0.7 reshape.358
  270.4 0.7 reshape.360
  272.1 0.7 reshape.364
  272.9 0.7 reshape.362
  273.6 1.0 all-to-all-done.7
  274.6 3.8 all-to-all-start.12
  278.6 5.2 %all-to-all-done.12 = bf16[8,2,512]{2,1,0:T(2,128)(2,1)S(1)} async-done(((bf16[8,2,512]{2,1,0:T(2,128)(2,1)}), bf16[8,2,512]{2,1,0:T(2,128)(2,1)S(1)}, u32[]{:S(2)}, u32[]{:S(2)}) %all-to-all-start.12) | async-done | bytes 16416 | tf_op jit(solution)/shard_map/all_to_all | solution.py:106
  283.8 3.3 all-to-all-start.10
  287.3 5.1 %all-to-all-done.10 = bf16[8,2,512]{2,1,0:T(2,128)(2,1)S(1)} async-done(((bf16[8,2,512]{2,1,0:T(2,128)(2,1)}), bf16[8,2,512]{2,1,0:T(2,128)(2,1)S(1)}, u32[]{:S(2)}, u32[]{:S(2)}) %all-to-all-start.10) | async-done | bytes 16416 | tf_op jit(solution)/shard_map/all_to_all | solution.py:103
  292.4 3.3 all-to-all-start.8
  295.9 5.2 %all-to-all-done.8 = bf16[8,2,512]{2,1,0:T(2,128)(2,1)S(1)} async-done(((bf16[8,2,512]{2,1,0:T(2,128)(2,1)}), bf16[8,2,512]{2,1,0:T(2,128)(2,1)S(1)}, u32[]{:S(2)}, u32[]{:S(2)}) %all-to-all-start.8) | async-done | bytes 16416 | tf_op jit(solution)/shard_map/all_to_all | solution.py:102
  301.0 3.3 all-to-all-start.11
  304.5 5.2 %all-to-all-done.11 = bf16[8,2,512]{2,1,0:T(2,128)(2,1)S(1)} async-done(((bf16[8,2,512]{2,1,0:T(2,128)(2,1)}), bf16[8,2,512]{2,1,0:T(2,128)(2,1)S(1)}, u32[]{:S(2)}, u32[]{:S(2)}) %all-to-all-start.11) | async-done | bytes 16416 | tf_op jit(solution)/shard_map/all_to_all | solution.py:101
  309.6 3.3 all-to-all-start.9
  313.9 4.3 %all-to-all-done.9 = bf16[8,2,512]{2,1,0:T(2,128)(2,1)S(1)} async-done(((bf16[8,2,512]{2,1,0:T(2,128)(2,1)}), bf16[8,2,512]{2,1,0:T(2,128)(2,1)S(1)}, u32[]{:S(2)}, u32[]{:S(2)}) %all-to-all-start.9) | async-done | bytes 16416 | tf_op jit(solution)/shard_map/all_to_all | solution.py:105
  319.0 3.4 fusion.11
  322.5 4.2 %fusion.15 = f32[32,4,1,64]{3,2,1,0:T(1,128)S(1)} fusion(bf16[32,4,64,1]{2,3,1,0:T(2,128)(2,1)S(1)} %reshape.321, f32[2,32,4,64,64]{4,3,2,1,0:T(8,128)} %param.27, f32[32,4,64]{2,1,0:T(4,128)S(1)} %get-tuple-element.27, f32[32,4,64]{2,1,0:T(4,128)S(1)} %reshape.307, f32[32,4,64]{2,1,0:T(4,128)S(1)} %get-tuple-element.26, f32[32,4,64]{2,1,0:T(4,128)S(1)} %bitcast.141, ...), kind=kOutput, calls=%fused_computation.24 | convolution fusion | flops 4194304 | bytes 4407328 | tf_op jit(solution)/shard_map/bhij,bhj->bhi/dot_general | solution.py:51
  327.3 12.7 %all_gather.45 = bf16[256,256]{1,0:T(8,128)(2,1)S(1)} all-gather(bf16[32,256]{1,0:T(8,128)(2,1)S(1)} %select_convert_fusion), channel_id=1, replica_groups=mesh['tp_0'=4,'tp_1'=4,'dp'=8] {'dp'}, dimensions={0}, use_global_device_ids=true | all-gather | bytes 147456 | tf_op jit(solution)/shard_map/all_gather | solution.py:121
  340.1 13.9 %all_gather.46 = bf16[256,1024]{1,0:T(8,128)(2,1)} all-gather(bf16[256,256]{1,0:T(8,128)(2,1)S(1)} %all_gather.45), channel_id=1, replica_groups=mesh['tp_0'=4,'tp_1'=4,'dp'=8] {'tp_1'}, dimensions={1}, use_global_device_ids=true | all-gather | bytes 655360 | tf_op jit(solution)/shard_map/all_gather | solution.py:19
  354.0 10.6 %add_select_fusion.1 = (f32[1,32,4,64,64]{4,3,2,1,0:T(8,128)}, f32[1,32,4,64,64]{4,3,2,1,0:T(8,128)}) fusion(f32[2,32,4,64,64]{4,3,2,1,0:T(8,128)} %param.27, f32[32,4,64]{2,1,0:T(4,128)S(1)} %get-tuple-element.29, f32[32,4,64]{2,1,0:T(4,128)S(1)} %reshape.301, f32[32,4,64]{2,1,0:T(4,128)S(1)} %get-tuple-element.28, f32[32,4,64]{2,1,0:T(4,128)S(1)} %bitcast.140, ...), kind=kLoop, calls=%fused_computation.26 | loop fusion | flops 6291456 | bytes 8716320 | tf_op jit(solution)/shard_map/jit(_where)/select_n | solution.py:50
  364.6 18.4 %all-gather.11.cloned.1.call-done = bf16[256,4096]{1,0:T(8,128)(2,1)} async-done(((bf16[256,1024]{1,0:T(8,128)(2,1)}), bf16[256,4096]{1,0:T(8,128)(2,1)}) %all-gather.11.cloned.1.call-update) | async-done | bytes 2097168 | tf_op jit(solution)/shard_map/all_gather | solution.py:19
  383.1 2.3 convolution_convert_fusion
  386.2 4.3 %all-to-all-start.13 = ((bf16[8,2,512]{2,1,0:T(2,128)(2,1)}), bf16[8,2,512]{2,1,0:T(2,128)(2,1)S(1)}, u32[]{:S(2)}, u32[]{:S(2)}) async-start(bf16[8,2,512]{2,1,0:T(2,128)(2,1)} %reshape.370), calls=%async_computation.13 | async-start | bytes 32768 | tf_op jit(solution)/shard_map/all_to_all | solution.py:130
  390.5 8.8 %pad_maximum_fusion = f32[2,32,4,64,64]{4,3,2,1,0:T(8,128)} fusion(f32[1,32,4,64,64]{4,3,2,1,0:T(8,128)} %get-tuple-element.13, f32[1,32,4,64,64]{4,3,2,1,0:T(8,128)} %get-tuple-element.12), kind=kLoop, calls=%fused_computation | loop fusion | flops 1048576 | bytes 8388608 | tf_op jit(solution)/shard_map/stack | solution.py:131
  (135 shorter events, 13.4 us)
Async XLA Ops:
  7.2 34.0 %copy-start.7 = (s32[32]{0:T(128)S(1)}, s32[32]{0:T(128)}, u32[]{:S(2)}) copy-start(s32[32]{0:T(128)} %param.15) | copy-start | bytes 388
  7.2 34.0 %copy-start.4 = (f32[2,256]{1,0:T(2,128)S(1)}, f32[2,256]{1,0:T(2,128)}, u32[]{:S(2)}) copy-start(f32[2,256]{1,0:T(2,128)} %param.26) | copy-start | bytes 6148
  7.2 34.0 %copy-start.1 = (bf16[2,4096,32]{1,2,0:T(8,128)(2,1)S(1)}, bf16[2,4096,32]{1,2,0:T(8,128)(2,1)}, u32[]{:S(2)}) copy-start(bf16[2,4096,32]{1,2,0:T(8,128)(2,1)} %param.20) | copy-start | bytes 1572868
  7.2 34.7 %copy-start.2 = (bf16[2,4096,32]{1,2,0:T(8,128)(2,1)S(1)}, bf16[2,4096,32]{1,2,0:T(8,128)(2,1)}, u32[]{:S(2)}) copy-start(bf16[2,4096,32]{1,2,0:T(8,128)(2,1)} %param.21) | copy-start | bytes 1572868
  7.2 35.5 %copy-start.3 = (bf16[2,4096,32]{1,2,0:T(8,128)(2,1)S(1)}, bf16[2,4096,32]{1,2,0:T(8,128)(2,1)}, u32[]{:S(2)}) copy-start(bf16[2,4096,32]{1,2,0:T(8,128)(2,1)} %param.22) | copy-start | bytes 1572868
  7.2 60.2 %all-gather.5.cloned.1.call-start = ((), (), s32[]{:S(2)}) async-start(), calls=%async_computation.14 | async-start | bytes 2621440 | tf_op jit(solution)/shard_map/all_gather | solution.py:19
  43.4 33.8 %copy-start.5 = (f32[2,256]{1,0:T(2,128)S(1)}, f32[2,256]{1,0:T(2,128)}, u32[]{:S(2)}) copy-start(f32[2,256]{1,0:T(2,128)} %param.25) | copy-start | bytes 6148
  43.4 33.8 %copy-start.6 = (f32[2,256]{1,0:T(2,128)S(1)}, f32[2,256]{1,0:T(2,128)}, u32[]{:S(2)}) copy-start(f32[2,256]{1,0:T(2,128)} %param.24) | copy-start | bytes 6148
  72.9 9.6 %all-to-all-start = ((bf16[8,2,512]{2,1,0:T(2,128)(2,1)}), bf16[8,2,512]{2,1,0:T(2,128)(2,1)S(1)}, u32[]{:S(2)}, u32[]{:S(2)}) async-start(bf16[8,2,512]{2,1,0:T(2,128)(2,1)} %reshape.354), calls=%async_computation | async-start | bytes 32768 | tf_op jit(solution)/shard_map/all_to_all | solution.py:104
  82.6 9.2 %all-to-all-start.5 = ((bf16[8,2,512]{2,1,0:T(2,128)(2,1)}), bf16[8,2,512]{2,1,0:T(2,128)(2,1)S(1)}, u32[]{:S(2)}, u32[]{:S(2)}) async-start(bf16[8,2,512]{2,1,0:T(2,128)(2,1)} %reshape.344), calls=%async_computation.5 | async-start | bytes 32768 | tf_op jit(solution)/shard_map/all_to_all | solution.py:106
  91.8 8.6 %all-to-all-start.3 = ((bf16[8,2,512]{2,1,0:T(2,128)(2,1)}), bf16[8,2,512]{2,1,0:T(2,128)(2,1)S(1)}, u32[]{:S(2)}, u32[]{:S(2)}) async-start(bf16[8,2,512]{2,1,0:T(2,128)(2,1)} %reshape.352), calls=%async_computation.3 | async-start | bytes 32768 | tf_op jit(solution)/shard_map/all_to_all | solution.py:103
  100.4 8.6 %all-to-all-start.1 = ((bf16[8,2,512]{2,1,0:T(2,128)(2,1)}), bf16[8,2,512]{2,1,0:T(2,128)(2,1)S(1)}, u32[]{:S(2)}, u32[]{:S(2)}) async-start(bf16[8,2,512]{2,1,0:T(2,128)(2,1)} %reshape.348), calls=%async_computation.1 | async-start | bytes 32768 | tf_op jit(solution)/shard_map/all_to_all | solution.py:102
  109.0 8.6 %all-to-all-start.4 = ((bf16[8,2,512]{2,1,0:T(2,128)(2,1)}), bf16[8,2,512]{2,1,0:T(2,128)(2,1)S(1)}, u32[]{:S(2)}, u32[]{:S(2)}) async-start(bf16[8,2,512]{2,1,0:T(2,128)(2,1)} %reshape.346), calls=%async_computation.4 | async-start | bytes 32768 | tf_op jit(solution)/shard_map/all_to_all | solution.py:101
  117.6 8.6 %all-to-all-start.2 = ((bf16[8,2,512]{2,1,0:T(2,128)(2,1)}), bf16[8,2,512]{2,1,0:T(2,128)(2,1)S(1)}, u32[]{:S(2)}, u32[]{:S(2)}) async-start(bf16[8,2,512]{2,1,0:T(2,128)(2,1)} %reshape.350), calls=%async_computation.2 | async-start | bytes 32768 | tf_op jit(solution)/shard_map/all_to_all | solution.py:105
  120.9 70.1 %all-gather.7.cloned.1.call-start = ((), (), s32[]{:S(2)}) async-start(), calls=%async_computation.15 | async-start | bytes 2621440 | tf_op jit(solution)/shard_map/all_gather | solution.py:19
  130.4 60.6 %copy-start = (bf16[2,4096,32]{1,2,0:T(8,128)(2,1)S(1)}, bf16[2,4096,32]{1,2,0:T(8,128)(2,1)}, u32[]{:S(2)}) copy-start(bf16[2,4096,32]{1,2,0:T(8,128)(2,1)} %param.23) | copy-start | bytes 1572868
  162.0 97.1 %all-gather.9.cloned.1.call-start = ((), (), s32[]{:S(2)}) async-start(), calls=%async_computation.16 | async-start | bytes 2621440 | tf_op jit(solution)/shard_map/all_gather | solution.py:19
  265.0 9.6 %all-to-all-start.7 = ((bf16[8,2,512]{2,1,0:T(2,128)(2,1)}), bf16[8,2,512]{2,1,0:T(2,128)(2,1)S(1)}, u32[]{:S(2)}, u32[]{:S(2)}) async-start(bf16[8,2,512]{2,1,0:T(2,128)(2,1)} %reshape.368), calls=%async_computation.7 | async-start | bytes 32768 | tf_op jit(solution)/shard_map/all_to_all | solution.py:104
  274.6 9.2 %all-to-all-start.12 = ((bf16[8,2,512]{2,1,0:T(2,128)(2,1)}), bf16[8,2,512]{2,1,0:T(2,128)(2,1)S(1)}, u32[]{:S(2)}, u32[]{:S(2)}) async-start(bf16[8,2,512]{2,1,0:T(2,128)(2,1)} %reshape.358), calls=%async_computation.12 | async-start | bytes 32768 | tf_op jit(solution)/shard_map/all_to_all | solution.py:106
  283.8 8.6 %all-to-all-start.10 = ((bf16[8,2,512]{2,1,0:T(2,128)(2,1)}), bf16[8,2,512]{2,1,0:T(2,128)(2,1)S(1)}, u32[]{:S(2)}, u32[]{:S(2)}) async-start(bf16[8,2,512]{2,1,0:T(2,128)(2,1)} %reshape.366), calls=%async_computation.10 | async-start | bytes 32768 | tf_op jit(solution)/shard_map/all_to_all | solution.py:103
  292.4 8.6 %all-to-all-start.8 = ((bf16[8,2,512]{2,1,0:T(2,128)(2,1)}), bf16[8,2,512]{2,1,0:T(2,128)(2,1)S(1)}, u32[]{:S(2)}, u32[]{:S(2)}) async-start(bf16[8,2,512]{2,1,0:T(2,128)(2,1)} %reshape.362), calls=%async_computation.8 | async-start | bytes 32768 | tf_op jit(solution)/shard_map/all_to_all | solution.py:102
  301.0 8.6 %all-to-all-start.11 = ((bf16[8,2,512]{2,1,0:T(2,128)(2,1)}), bf16[8,2,512]{2,1,0:T(2,128)(2,1)S(1)}, u32[]{:S(2)}, u32[]{:S(2)}) async-start(bf16[8,2,512]{2,1,0:T(2,128)(2,1)} %reshape.360), calls=%async_computation.11 | async-start | bytes 32768 | tf_op jit(solution)/shard_map/all_to_all | solution.py:101
  309.6 8.6 %all-to-all-start.9 = ((bf16[8,2,512]{2,1,0:T(2,128)(2,1)}), bf16[8,2,512]{2,1,0:T(2,128)(2,1)S(1)}, u32[]{:S(2)}, u32[]{:S(2)}) async-start(bf16[8,2,512]{2,1,0:T(2,128)(2,1)} %reshape.364), calls=%async_computation.9 | async-start | bytes 32768 | tf_op jit(solution)/shard_map/all_to_all | solution.py:105
  313.0 70.1 %all-gather.11.cloned.1.call-start = ((), (), s32[]{:S(2)}) async-start(), calls=%async_computation.17 | async-start | bytes 2621440 | tf_op jit(solution)/shard_map/all_gather | solution.py:19
  386.2 13.0 %all-to-all-start.13 = ((bf16[8,2,512]{2,1,0:T(2,128)(2,1)}), bf16[8,2,512]{2,1,0:T(2,128)(2,1)S(1)}, u32[]{:S(2)}, u32[]{:S(2)}) async-start(bf16[8,2,512]{2,1,0:T(2,128)(2,1)} %reshape.370), calls=%async_computation.13 | async-start | bytes 32768 | tf_op jit(solution)/shard_map/all_to_all | solution.py:130
Sparse Core Ops, SparseCore 0:
  35.1 32.3 all-gather.4
  162.1 28.8 all-gather.6
  230.1 28.8 all-gather.8
  354.1 28.8 all-gather.10
where the time goes:
time: 410 us; the launch traced here: 407 us
  waiting for transfers between devices  152 us (37%)
  blocking collectives  117 us (29%)
  starting transfers between devices  47.2 us (12%)
  other arithmetic  25.6 us (6%)
  matrix products  25.2 us (6%)
  local copies, waits for them, and re-layouts  24.6 us (6%)
  between operations  14.4 us (4%)
    all_gather x4, waiting for transfers between devices, gather_axes(): nearer = lax.all_gather(value, axes[-1], axis=dim, tiled=True)  101 us
    all_gather x4, blocking collectives, gather_axes(): nearer = lax.all_gather(value, axes[-1], axis=dim, tiled=True)  55.9 us
    all_gather x2, blocking collectives, local(): batch_raw = lax.all_gather(current, 'dp', axis=0, tiled=True)  26.3 us
    all_gather x2, blocking collectives, local(): rows_all = lax.all_gather(mixed_here, 'dp', axis=0, tiled=True)  25.5 us
    unnamed x50, local copies, waits for them, and re-layouts  18.4 us
    select_n x1, other arithmetic, recur(): updated = jnp.where(active[:, None, None, None], updated, state_old)  10.6 us
    all_to_all x2, waiting for transfers between devices, local(): lax.all_to_all(shortened(pieces[5]), 'dp', split_axis=0, concat_axis=1, t...  10.5 us
    all_to_all x2, waiting for transfers between devices, local(): lax.all_to_all(shortened(pieces[1]), 'dp', split_axis=0, concat_axis=1, t...  10.3 us
  transfers between devices with their start and end apart: 17, of which 16 were waited for; matrix products, arithmetic and copies ran while one was open for 10% of the time, Pallas kernels for 0%

commit v1 on v0

v1 whole, which is shorter than its diff:
```python
import functools

import jax
import jax.numpy as jnp
from jax import lax
from jax.experimental import pallas as pl
from jax.experimental.pallas import tpu as pltpu
from jax.sharding import PartitionSpec as P

STEP = 16
RMS_EPS = 1e-06
GROUP_EPS = 0.00064
MESH = pl.DeviceIdType.MESH
F32 = jnp.float32
BF16 = jnp.bfloat16
ORDERS = (("x", "y", "z"), ("y", "z", "x"), ("z", "x", "y"), ("y", "x", "z"))
LANES = (((1,), (1,)), ((), ()))
PLAIN = (((1,), (0,)), ((), ()))
ROWS = (((0,), (0,)), ((), ()))


def step_kernel(
    tok, lens, gain, w0, w1, w2, w3, w4, w5, w_out, dbase, rbase, ggain, state,
    mixed, sa_out, v_out, pq_out, dec_out,
    G, WP, WO, ST, SB, RB, FB, FR, V8, M2,
    g_send, g_recv, a_send, a_recv, w_local, w_send, w_recv, st_sem, tok_sem,
):
    tp, dp = lax.axis_index("tp"), lax.axis_index("dp")
    c = dp % 2
    at = {"z": tp // 4, "y": tp % 4, "x": dp // 2}
    projections = (w0, w1, w2, w3, w4, w5)

    def device(axis, hop):
        to = dict(at)
        to[axis] = (at[axis] + hop) % 4
        return (to["z"] * 4 + to["y"], to["x"] * 2 + c)

    partner = (tp, at["x"] * 2 + 1 - c)

    barrier = pltpu.get_barrier_semaphore()
    for axis in "xyz":
        for hop in (1, 2, 3):
            pl.semaphore_signal(barrier, inc=1, device_id=device(axis, hop), device_id_type=MESH)
    pl.semaphore_signal(barrier, inc=1, device_id=partner, device_id_type=MESH)

    tok_copies = []
    for q in range(4):
        rh, ch = q // 2, q % 2
        tok_copies.append(pltpu.make_async_copy(
            tok.at[pl.ds(rh * 16, 16), pl.ds(ch * 128, 128)],
            G.at[0, q, at["z"], at["y"], at["x"]],
            tok_sem.at[q],
        ))
        tok_copies[-1].start()
    mine = pl.multiple_of(c * 32, 32)
    for layer in range(2):
        for kind in range(6):
            pltpu.make_async_copy(
                projections[kind].at[layer],
                WP.at[layer, pl.ds(kind * 64 + mine, 32)],
                w_local.at[layer, 0],
            ).start()
        pltpu.make_async_copy(
            w_out.at[layer], WO.at[layer, pl.ds(mine, 32)], w_local.at[layer, 1]
        ).start()
        pltpu.make_async_copy(state.at[layer], ST.at[layer], st_sem.at[layer]).start()

    pl.semaphore_wait(barrier, 10)

    def block(a, q, free, moved=None):
        idx = [moved[ax] if moved and ax in moved else at[ax] for ax in "zyx"]
        idx = [slice(None) if ax in free else i for ax, i in zip("zyx", idx)]
        return G.at[(a, q, *idx)]

    def send(ref, axis, hop, send_sem, recv_sem):
        pltpu.make_async_remote_copy(
            src_ref=ref, dst_ref=ref, send_sem=send_sem, recv_sem=recv_sem,
            device_id=device(axis, hop), device_id_type=MESH,
        ).start()

    def landed(ref, sem):
        pltpu.make_async_copy(ref, ref, sem).wait()

    def gather_first(a):
        for q in range(4):
            if a == 0:
                tok_copies[q].wait()
            for hop in (1, 2, 3):
                send(block(a, q, ()), ORDERS[q][0], hop, g_send.at[a, q, 0], g_recv.at[a, q, 0])

    def gather_middle(a):
        for q in range(4):
            first, second, third = ORDERS[q]
            landed(G.at[a, q, 0, 0, pl.ds(0, 3)], g_recv.at[a, q, 0])
            for hop in (2, 1, 3):
                send(block(a, q, first), second, hop, g_send.at[a, q, 1], g_recv.at[a, q, hop])
            for hop in (2, 1, 3):
                send(block(a, q, first), third, hop, g_send.at[a, q, 2], g_recv.at[a, q, 4])
        for hop in (1, 3, 2):
            for q in range(4):
                first, second, third = ORDERS[q]
                landed(G.at[a, q, 0, 0], g_recv.at[a, q, hop])
                line = {second: (at[second] + 4 - hop) % 4}
                for on in (2, 1, 3):
                    send(block(a, q, first, line), third, on, g_send.at[a, q, 2], g_recv.at[a, q, 4])

    def gather_last(a):
        for q in range(4):
            landed(G.at[a, q, pl.ds(0, 3)], g_recv.at[a, q, 4])

    def gather_sent(a):
        for q in range(4):
            landed(G.at[a, q, 0, 0, pl.ds(0, 3)], g_send.at[a, q, 0])
            landed(G.at[a, q, pl.ds(0, 3), :, 0], g_send.at[a, q, 1])
            landed(G.at[a, q, pl.ds(0, 3)], g_send.at[a, q, 2])

    def rows_chunk(a, z):
        parts = []
        for y in range(4):
            for ch in range(2):
                halves = [G[a, rh * 2 + ch, z, y].reshape(64, 128) for rh in range(2)]
                parts.append(jnp.concatenate(halves, axis=0))
        return parts

    def exchange(n, src, dst):
        for hop in (2, 1, 3):
            to = (at["x"] + hop) % 4
            pltpu.make_async_remote_copy(
                src_ref=src.at[to], dst_ref=dst.at[at["x"]],
                send_sem=a_send.at[n], recv_sem=a_recv.at[n],
                device_id=device("x", hop), device_id_type=MESH,
            ).start()
        dst[at["x"]] = src[at["x"]]
        landed(dst.at[pl.ds(0, 3)], a_recv.at[n])

    def exchange_sent(n, src):
        landed(src.at[pl.ds(0, 3)], a_send.at[n])

    def weights_out():
        for layer in range(2):
            for kind in range(6):
                pltpu.make_async_remote_copy(
                    src_ref=projections[kind].at[layer],
                    dst_ref=WP.at[layer, pl.ds(kind * 64 + mine, 32)],
                    send_sem=w_send.at[layer, 0], recv_sem=w_recv.at[layer, 0],
                    device_id=partner, device_id_type=MESH,
                ).start()
            pltpu.make_async_remote_copy(
                src_ref=w_out.at[layer],
                dst_ref=WO.at[layer, pl.ds(mine, 32)],
                send_sem=w_send.at[layer, 1], recv_sem=w_recv.at[layer, 1],
                device_id=partner, device_id_type=MESH,
            ).start()

    def weights_in(layer):
        landed(WP.at[layer, pl.ds(0, 192)], w_local.at[layer, 0])
        landed(WP.at[layer, pl.ds(0, 192)], w_recv.at[layer, 0])
        landed(WO.at[layer, pl.ds(0, 32)], w_local.at[layer, 1])
        landed(WO.at[layer, pl.ds(0, 32)], w_recv.at[layer, 1])
        scale = gain[layer:layer + 1, :]

        def fold(i, carry):
            rows = pl.ds(pl.multiple_of(i * 16, 16), 16)
            WP[layer, rows, :] = (WP[layer, rows, :].astype(F32) * scale).astype(BF16)
            return carry

        lax.fori_loop(0, 24, fold, 0)

    def weights_sent():
        for layer in range(2):
            landed(WP.at[layer, pl.ds(0, 192)], w_send.at[layer, 0])
            landed(WO.at[layer, pl.ds(0, 32)], w_send.at[layer, 1])

    def put_projected(layer, projected):
        out = projected.astype(BF16)
        for to in range(4):
            SB[layer, to, 0:16, :] = out[to * 16:to * 16 + 16, :]
            SB[layer, to, 16:32, :] = out[64 + to * 16:64 + to * 16 + 16, :]

    def project_first():
        acc = jnp.zeros((128, 384), F32)
        squares = jnp.zeros((128, 128), F32)
        for z in range(4):
            parts = rows_chunk(0, z)
            for part in parts:
                wide = part.astype(F32)
                squares += wide * wide
            acc += lax.dot_general(
                jnp.concatenate(parts, axis=1), WP[0, :, z * 1024:(z + 1) * 1024], LANES,
                preferred_element_type=F32,
            )
        factor = lax.rsqrt(jnp.sum(squares, axis=1, keepdims=True) * (1.0 / 4096) + RMS_EPS)
        put_projected(0, acc * factor)

    def project_second():
        acc = jnp.zeros((384, 128), F32)
        squares = jnp.zeros((16, 128), F32)
        for z in range(4):
            parts = [G[2, q, z, y, x] for y in range(4) for x in range(4) for q in range(4)]
            for part in parts:
                wide = part.astype(F32)
                squares += wide * wide
            acc += lax.dot_general(
                WP[1, :, z * 1024:(z + 1) * 1024], jnp.concatenate(parts, axis=0), PLAIN,
                preferred_element_type=F32,
            )
        factor = lax.rsqrt(jnp.sum(squares, axis=0, keepdims=True) * (1.0 / 4096) + RMS_EPS)
        put_projected(1, (acc * factor).T)

    ident = lax.broadcasted_iota(jnp.int32, (32, 32), 0) == lax.broadcasted_iota(jnp.int32, (32, 32), 1)
    length = jnp.sum(jnp.where(ident, jnp.broadcast_to(lens[0:1, :], (32, 32)), 0), axis=1, keepdims=True)
    active = length > STEP

    def wide128(value):
        return jnp.concatenate([value, jnp.zeros_like(value)], axis=1)

    def recur(layer, a):
        values, gates, first_sums, second_sums = [], [], [], []
        for h in range(4):
            take = lambda kind: RB[layer, h, :, kind * 64:(kind + 1) * 64].astype(F32)
            recept, key, value, dpre, rpre, gpre = [take(kind) for kind in range(6)]
            cols = slice(h * 64, (h + 1) * 64)
            decay = jnp.exp(-(0.6065306597126334 * jax.nn.sigmoid(dbase[layer:layer + 1, cols] + dpre)))
            rate = jax.nn.sigmoid(rbase[layer:layer + 1, cols] + rpre)
            norm = jnp.sqrt(jnp.sum(key * key, axis=1, keepdims=True))
            unit = key / jnp.maximum(norm, 1e-12)
            up, kp = unit * rate, key * rate
            first_sums.append(jnp.broadcast_to(jnp.sum(up * recept, axis=1, keepdims=True), (32, 64)))
            second_sums.append(jnp.broadcast_to(jnp.sum(kp * recept, axis=1, keepdims=True), (32, 64)))
            values.append(value)
            gates.append(jax.nn.sigmoid(gpre))
            V8[pl.ds(h, 32, stride=8), :] = wide128(-unit)
            V8[pl.ds(4 + h, 32, stride=8), :] = wide128(decay * recept)
            pq_out[layer, pl.ds(h, 32, stride=8), :] = wide128(jnp.where(active, up, 0.0))
            pq_out[layer, pl.ds(4 + h, 32, stride=8), :] = wide128(jnp.where(active, kp, 0.0))
            dec_out[layer, pl.ds(h, 32, stride=8), :] = wide128(jnp.where(active, decay, 1.0))
            dec_out[layer, pl.ds(4 + h, 32, stride=8), :] = jnp.zeros((32, 128), F32)
        for b in range(32):
            got = lax.dot_general(
                V8[b * 8:(b + 1) * 8, 0:64].astype(BF16),
                ST[layer, b].reshape(256, 64).astype(BF16), LANES,
                preferred_element_type=F32,
            )
            for half in range(2):
                M2[half, b * 8:(b + 1) * 8, :] = got[:, half * 128:(half + 1) * 128]
        low = lax.broadcasted_iota(jnp.int32, (32, 128), 1) < 64

        def heads(base):
            return jnp.concatenate([
                jnp.where(low, M2[half, pl.ds(base + 2 * half, 32, stride=8), :],
                          M2[half, pl.ds(base + 2 * half + 1, 32, stride=8), :])
                for half in range(2)
            ], axis=1)

        sa, direct = heads(0), heads(4)
        value = jnp.concatenate(values, axis=1)
        sa_out[layer] = sa
        v_out[layer] = value
        readout = direct + sa * jnp.concatenate(first_sums, axis=1) + value * jnp.concatenate(second_sums, axis=1)
        normal = []
        for h in range(4):
            seg = readout[:, h * 64:(h + 1) * 64]
            seg = seg - jnp.sum(seg, axis=1, keepdims=True) * (1.0 / 64)
            spread = jnp.sum(seg * seg, axis=1, keepdims=True) * (1.0 / 64)
            normal.append(seg * lax.rsqrt(spread + GROUP_EPS))
        rows = jnp.concatenate(normal, axis=1) * ggain[layer:layer + 1, :] * jnp.concatenate(gates, axis=1)
        rows = jnp.where(active, rows, 0.0).astype(BF16)
        for q in range(4):
            rh, ch = q // 2, q % 2
            G[a, q, at["z"], at["y"], at["x"]] = rows[rh * 16:(rh + 1) * 16, ch * 128:(ch + 1) * 128]

    gather_first(0)
    weights_out()
    gather_middle(0)
    weights_in(0)
    gather_last(0)
    project_first()
    exchange(0, SB.at[0], RB.at[0])
    landed(ST.at[0], st_sem.at[0])
    recur(0, 1)

    gather_first(1)
    gather_middle(1)
    weights_in(1)
    gather_last(1)
    acc = jnp.zeros((64, 128), F32)
    for z in range(4):
        acc += lax.dot_general(
            WO[0, :, z * 1024:(z + 1) * 1024], jnp.concatenate(rows_chunk(1, z), axis=1), LANES,
            preferred_element_type=F32,
        )
    out = acc.astype(BF16)
    for q in range(4):
        G[2, q, at["z"], at["y"], at["x"]] = out[q * 16:(q + 1) * 16, :]

    gather_first(2)
    gather_middle(2)
    gather_last(2)
    project_second()
    exchange(1, SB.at[1], RB.at[1])
    landed(ST.at[1], st_sem.at[1])
    recur(1, 3)

    gather_first(3)
    gather_middle(3)
    gather_last(3)
    acc = jnp.zeros((128, 64), F32)
    for z in range(4):
        acc += lax.dot_general(
            jnp.concatenate(rows_chunk(3, z), axis=1), WO[1, :, z * 1024:(z + 1) * 1024], LANES,
            preferred_element_type=F32,
        )
    out = wide128(acc).astype(BF16)
    for to in range(4):
        FB[to, 0:16, :] = out[to * 16:to * 16 + 16, :]
        FB[to, 16:32, :] = out[64 + to * 16:64 + to * 16 + 16, :]
    exchange(2, FB, FR)
    mixed[...] = jnp.concatenate([FR[h, :, 0:64] for h in range(4)], axis=1)

    for a in range(4):
        gather_sent(a)
    exchange_sent(0, SB.at[0])
    exchange_sent(1, SB.at[1])
    exchange_sent(2, FB)
    weights_sent()


def update_kernel(state, sa, val, pq, dec, out):
    own = lax.broadcasted_iota(jnp.int32, (8, 256), 1) // 64
    row = lax.broadcasted_iota(jnp.int32, (8, 256), 0)
    for b in range(8):
        left = jnp.where(row < 4, jnp.broadcast_to(sa[0, b:b + 1, :], (8, 256)),
                         jnp.broadcast_to(val[0, b:b + 1, :], (8, 256)))
        left = jnp.where(row % 4 == own, left, 0.0)
        delta = lax.dot_general(
            left.astype(BF16), pq[0, b * 8:(b + 1) * 8, 0:64].astype(BF16), ROWS,
            preferred_element_type=F32,
        )
        for h in range(4):
            out[0, b, h] = state[0, b, h] * dec[0, b * 8 + h:b * 8 + h + 1, 0:64] + delta[h * 64:(h + 1) * 64, :]


def local(tokens, lengths, norm_gain, w_recept, w_key, w_value, w_decay, w_rate, w_gate, w_out,
          decay_base, rate_base, group_gain, state):
    weights = [jnp.swapaxes(w, 1, 2) for w in (w_recept, w_key, w_value, w_decay, w_rate, w_gate, w_out)]
    any_spec = pl.BlockSpec(memory_space=pl.ANY)
    vmem = pl.BlockSpec(memory_space=pltpu.VMEM)
    mixed, sa, val, pq, dec = pl.pallas_call(
        step_kernel,
        out_shape=(
            jax.ShapeDtypeStruct((32, 256), BF16),
            jax.ShapeDtypeStruct((2, 32, 256), F32),
            jax.ShapeDtypeStruct((2, 32, 256), F32),
            jax.ShapeDtypeStruct((2, 256, 128), F32),
            jax.ShapeDtypeStruct((2, 256, 128), F32),
        ),
        in_specs=[any_spec, vmem, vmem] + [any_spec] * 7 + [vmem] * 3 + [any_spec],
        out_specs=(vmem,) * 5,
        scratch_shapes=[
            pltpu.VMEM((4, 4, 4, 4, 4, 16, 128), BF16),
            pltpu.VMEM((2, 384, 4096), BF16),
            pltpu.VMEM((2, 64, 4096), BF16),
            pltpu.VMEM((2, 32, 4, 64, 64), F32),
            pltpu.VMEM((2, 4, 32, 384), BF16),
            pltpu.VMEM((2, 4, 32, 384), BF16),
            pltpu.VMEM((4, 32, 128), BF16),
            pltpu.VMEM((4, 32, 128), BF16),
            pltpu.VMEM((256, 128), F32),
            pltpu.VMEM((2, 256, 128), F32),
            pltpu.SemaphoreType.DMA((4, 4, 3)),
            pltpu.SemaphoreType.DMA((4, 4, 5)),
            pltpu.SemaphoreType.DMA((3,)),
            pltpu.SemaphoreType.DMA((3,)),
            pltpu.SemaphoreType.DMA((2, 2)),
            pltpu.SemaphoreType.DMA((2, 2)),
            pltpu.SemaphoreType.DMA((2, 2)),
            pltpu.SemaphoreType.DMA((2,)),
            pltpu.SemaphoreType.DMA((4,)),
        ],
        compiler_params=pltpu.CompilerParams(collective_id=0, has_side_effects=True),
        name="decode_step",
    )(tokens, lengths.reshape(1, 32), norm_gain, *weights, decay_base, rate_base, group_gain, state)
    new_state = pl.pallas_call(
        update_kernel,
        grid=(2, 4),
        out_shape=jax.ShapeDtypeStruct(state.shape, F32),
        in_specs=[
            pl.BlockSpec((1, 8, 4, 64, 64), lambda l, i: (l, i, 0, 0, 0)),
            pl.BlockSpec((1, 8, 256), lambda l, i: (l, i, 0)),
            pl.BlockSpec((1, 8, 256), lambda l, i: (l, i, 0)),
            pl.BlockSpec((1, 64, 128), lambda l, i: (l, i, 0)),
            pl.BlockSpec((1, 64, 128), lambda l, i: (l, i, 0)),
        ],
        out_specs=pl.BlockSpec((1, 8, 4, 64, 64), lambda l, i: (l, i, 0, 0, 0)),
        name="state_update",
    )(state, sa, val, pq, dec)
    return mixed, new_state


def solution(mesh):
    both = P(None, None, ("tp", "dp"))
    in_specs = (
        P("dp", "tp"), P("dp"), P(), both, both, both, both, both, both, both,
        P(None, "tp"), P(None, "tp"), P(None, "tp"), P(None, "dp", "tp", None, None),
    )
    out_specs = (P("dp", "tp"), P(None, "dp", "tp", None, None))
    return jax.shard_map(local, mesh=mesh, in_specs=in_specs, out_specs=out_specs, check_vma=False)
```

time: 410 us -> 90.8 us (0.22)
  waiting for transfers between devices: 152 us -> 0 us
  blocking collectives: 117 us -> 0 us
  Pallas kernels: 0 us -> 89.1 us
  starting transfers between devices: 47.2 us -> 0 us
  other arithmetic: 25.6 us -> 0 us
  matrix products: 25.2 us -> 0 us
  local copies, waits for them, and re-layouts: 24.6 us -> 0.61 us
  between operations: 14.4 us -> 0.65 us
    all_gather x8 -> x0, blocking collectives: 108 us -> none  [the longest x4 55.9 us: gather_axes(): nearer = lax.all_gather(value, axes[-1], axis=dim, tiled=True)]
    all_gather x4 -> x0, waiting for transfers between devices: 101 us -> none  [gather_axes(): nearer = lax.all_gather(value, axes[-1], axis=dim, tiled=True)]
    pallas_call x0 -> x2, Pallas kernels: none -> 89.1 us  [the longest x1 78.9 us: local(): pl.pallas_call(step_kernel, out_shape=(jax.ShapeDtypeStruct((32, 256), BF...]
    all_to_all x13 -> x0, waiting for transfers between devices: 51.9 us -> none  [the longest x2 10.5 us: local(): lax.all_to_all(shortened(pieces[5]), 'dp', split_axis=0, concat_axis=1, t...]
    all_to_all x13 -> x0, starting transfers between devices: 47 us -> none  [the longest x2 8.51 us: local(): lax.all_to_all(shortened(pieces[3]), 'dp', split_axis=0, concat_axis=1, t...]
    dot_general x8 -> x0, matrix products: 25.2 us -> none  [the longest x2 8.39 us: recur(): jnp.einsum('bhij,bhj->bhi', updated, recept_h, precision=lax.Precision.DE...]
    unnamed x50 -> x3, local copies, waits for them, and re-layouts: 18.4 us -> 0.61 us
    select_n x1 -> x0, other arithmetic: 10.6 us -> none  [recur(): updated = jnp.where(active[:, None, None, None], updated, state_old)]
  transfers between devices with their start and end apart: 17 -> 0, of which waited for: 16 -> 0; matrix products, arithmetic and copies ran while one was open for 10% -> 0% of each run, Pallas kernels for 0% -> 0%
where the time goes in v1:
time: 90.8 us; the launch traced here: 90.4 us
  Pallas kernels  89.1 us (98%)
    pallas_call x1, Pallas kernels, local(): pl.pallas_call(step_kernel, out_shape=(jax.ShapeDtypeStruct((32, 256), BF...  78.9 us
    pallas_call x1, Pallas kernels, local(): pl.pallas_call(update_kernel, grid=(2, 4), out_shape=jax.ShapeDtypeStruct...  10.2 us

profile of v1, /device:TPU:0, one launch (start us, length us, event | category | flops | bytes accessed | tf_op | source)
XLA Modules:
  0.0 90.4 jit_solution(2831532444298282697)
XLA Ops:
  0.6 78.9 %decode_step.1 = (bf16[32,256]{1,0:T(8,128)(2,1)}, f32[2,32,256]{2,1,0:T(8,128)}, f32[2,32,256]{2,1,0:T(8,128)}, f32[2,256,128]{2,1,0:T(8,128)}, f32[2,256,128]{2,1,0:T(8,128)}) custom-call(bf16[32,256]{1,0:T(8,128)(2,1)} %tok.1, s32[1,32]{1,0:T(1,128)} %bitcast.15, f32[2,4096]{1,0:T(2,128)} %gain.1, bf16[2,32,4096]{2,1,0:T(8,128)(2,1)} %bitcast.8, ...), custom_call_target="tpu_custom_call" | custom-call | tf_op jit(solution)/shard_map/decode_step/pallas_call | solution.py:348
  79.6 0.0 copy-start
  79.6 10.2 %state_update.1 = f32[2,32,4,64,64]{4,3,2,1,0:T(8,128)} custom-call(f32[2,32,4,64,64]{4,3,2,1,0:T(8,128)} %state.3, f32[2,32,256]{2,1,0:T(8,128)} %get-tuple-element.8.sa, f32[2,32,256]{2,1,0:T(8,128)} %get-tuple-element.9.val, f32[2,256,128]{2,1,0:T(8,128)} %get-tuple-element.10.pq, f32[2,256,128]{2,1,0:T(8,128)} %get-tuple-element.11.dec), custom_call_target="tpu_custom_call" | custom-call | tf_op jit(solution)/shard_map/state_update/pallas_call | solution.py:383
  89.8 0.0 copy-done
  89.8 0.6 copy.17
Async XLA Ops:
  79.6 10.2 %copy-start = (bf16[32,256]{1,0:T(8,128)(2,1)S(1)}, bf16[32,256]{1,0:T(8,128)(2,1)}, u32[]{:S(2)}) copy-start(bf16[32,256]{1,0:T(8,128)(2,1)} %get-tuple-element.14) | copy-start | bytes 49156

commit v2 on v1

--- a/solution.py
+++ b/solution.py
@@ -21,8 +21,8 @@
 
 def step_kernel(
     tok, lens, gain, w0, w1, w2, w3, w4, w5, w_out, dbase, rbase, ggain, state,
-    mixed, sa_out, v_out, pq_out, dec_out,
-    G, WP, WO, ST, SB, RB, FB, FR, V8, M2,
+    mixed, ST,
+    G, WP, WO, SB, RB, FB, FR, V8, M2, SA, VA, PQ, DEC,
     g_send, g_recv, a_send, a_recv, w_local, w_send, w_recv, st_sem, tok_sem,
 ):
     tp, dp = lax.axis_index("tp"), lax.axis_index("dp")
@@ -41,7 +41,6 @@
     for axis in "xyz":
         for hop in (1, 2, 3):
             pl.semaphore_signal(barrier, inc=1, device_id=device(axis, hop), device_id_type=MESH)
-    pl.semaphore_signal(barrier, inc=1, device_id=partner, device_id_type=MESH)
 
     tok_copies = []
     for q in range(4):
@@ -63,9 +62,9 @@
         pltpu.make_async_copy(
             w_out.at[layer], WO.at[layer, pl.ds(mine, 32)], w_local.at[layer, 1]
         ).start()
-        pltpu.make_async_copy(state.at[layer], ST.at[layer], st_sem.at[layer]).start()
-
-    pl.semaphore_wait(barrier, 10)
+
+    pl.semaphore_wait(barrier, 9 + c)
+    pl.semaphore_signal(barrier, inc=1, device_id=partner, device_id_type=MESH)
 
     def block(a, q, free, moved=None):
         idx = [moved[ax] if moved and ax in moved else at[ax] for ax in "zyx"]
@@ -231,10 +230,9 @@
             gates.append(jax.nn.sigmoid(gpre))
             V8[pl.ds(h, 32, stride=8), :] = wide128(-unit)
             V8[pl.ds(4 + h, 32, stride=8), :] = wide128(decay * recept)
-            pq_out[layer, pl.ds(h, 32, stride=8), :] = wide128(jnp.where(active, up, 0.0))
-            pq_out[layer, pl.ds(4 + h, 32, stride=8), :] = wide128(jnp.where(active, kp, 0.0))
-            dec_out[layer, pl.ds(h, 32, stride=8), :] = wide128(jnp.where(active, decay, 1.0))
-            dec_out[layer, pl.ds(4 + h, 32, stride=8), :] = jnp.zeros((32, 128), F32)
+            PQ[pl.ds(h, 32, stride=8), :] = wide128(jnp.where(active, up, 0.0))
+            PQ[pl.ds(4 + h, 32, stride=8), :] = wide128(jnp.where(active, kp, 0.0))
+            DEC[pl.ds(h, 32, stride=8), :] = wide128(jnp.where(active, decay, 1.0))
         for b in range(32):
             got = lax.dot_general(
                 V8[b * 8:(b + 1) * 8, 0:64].astype(BF16),
@@ -254,8 +252,8 @@
 
         sa, direct = heads(0), heads(4)
         value = jnp.concatenate(values, axis=1)
-        sa_out[layer] = sa
-        v_out[layer] = value
+        SA[...] = sa
+        VA[...] = value
         readout = direct + sa * jnp.concatenate(first_sums, axis=1) + value * jnp.concatenate(second_sums, axis=1)
         normal = []
         for h in range(4):
@@ -269,9 +267,37 @@
             rh, ch = q // 2, q % 2
             G[a, q, at["z"], at["y"], at["x"]] = rows[rh * 16:(rh + 1) * 16, ch * 128:(ch + 1) * 128]
 
+    head_of = lax.broadcasted_iota(jnp.int32, (8, 256), 1) // 64
+    row_of = lax.broadcasted_iota(jnp.int32, (8, 256), 0)
+
+    def update(layer, start, count):
+        for b in range(start, start + count):
+            left = jnp.where(row_of < 4, jnp.broadcast_to(SA[b:b + 1, :], (8, 256)),
+                             jnp.broadcast_to(VA[b:b + 1, :], (8, 256)))
+            left = jnp.where(row_of % 4 == head_of, left, 0.0)
+            delta = lax.dot_general(
+                left.astype(BF16), PQ[b * 8:(b + 1) * 8, 0:64].astype(BF16), ROWS,
+                preferred_element_type=F32,
+            )
+            for h in range(4):
+                ST[layer, b, h] = (ST[layer, b, h] * DEC[b * 8 + h:b * 8 + h + 1, 0:64]
+                                   + delta[h * 64:(h + 1) * 64, :])
+
     gather_first(0)
-    weights_out()
+    for layer in range(2):
+        pltpu.make_async_copy(state.at[layer], ST.at[layer], st_sem.at[layer]).start()
+
+    @pl.when(c == 1)
+    def _():
+        weights_out()
+
     gather_middle(0)
+
+    @pl.when(c == 0)
+    def _():
+        pl.semaphore_wait(barrier, 1)
+        weights_out()
+
     weights_in(0)
     gather_last(0)
     project_first()
@@ -280,7 +306,9 @@
     recur(0, 1)
 
     gather_first(1)
+    update(0, 0, 10)
     gather_middle(1)
+    update(0, 10, 22)
     weights_in(1)
     gather_last(1)
     acc = jnp.zeros((64, 128), F32)
@@ -302,7 +330,9 @@
     recur(1, 3)
 
     gather_first(3)
+    update(1, 0, 10)
     gather_middle(3)
+    update(1, 10, 22)
     gather_last(3)
     acc = jnp.zeros((128, 64), F32)
     for z in range(4):
@@ -325,48 +355,30 @@
     weights_sent()
 
 
-def update_kernel(state, sa, val, pq, dec, out):
-    own = lax.broadcasted_iota(jnp.int32, (8, 256), 1) // 64
-    row = lax.broadcasted_iota(jnp.int32, (8, 256), 0)
-    for b in range(8):
-        left = jnp.where(row < 4, jnp.broadcast_to(sa[0, b:b + 1, :], (8, 256)),
-                         jnp.broadcast_to(val[0, b:b + 1, :], (8, 256)))
-        left = jnp.where(row % 4 == own, left, 0.0)
-        delta = lax.dot_general(
-            left.astype(BF16), pq[0, b * 8:(b + 1) * 8, 0:64].astype(BF16), ROWS,
-            preferred_element_type=F32,
-        )
-        for h in range(4):
-            out[0, b, h] = state[0, b, h] * dec[0, b * 8 + h:b * 8 + h + 1, 0:64] + delta[h * 64:(h + 1) * 64, :]
-
-
 def local(tokens, lengths, norm_gain, w_recept, w_key, w_value, w_decay, w_rate, w_gate, w_out,
           decay_base, rate_base, group_gain, state):
     weights = [jnp.swapaxes(w, 1, 2) for w in (w_recept, w_key, w_value, w_decay, w_rate, w_gate, w_out)]
-    any_spec = pl.BlockSpec(memory_space=pl.ANY)
+    hbm = pl.BlockSpec(memory_space=pltpu.HBM)
     vmem = pl.BlockSpec(memory_space=pltpu.VMEM)
-    mixed, sa, val, pq, dec = pl.pallas_call(
+    mixed, new_state = pl.pallas_call(
         step_kernel,
-        out_shape=(
-            jax.ShapeDtypeStruct((32, 256), BF16),
-            jax.ShapeDtypeStruct((2, 32, 256), F32),
-            jax.ShapeDtypeStruct((2, 32, 256), F32),
-            jax.ShapeDtypeStruct((2, 256, 128), F32),
-            jax.ShapeDtypeStruct((2, 256, 128), F32),
-        ),
-        in_specs=[any_spec, vmem, vmem] + [any_spec] * 7 + [vmem] * 3 + [any_spec],
-        out_specs=(vmem,) * 5,
+        out_shape=(jax.ShapeDtypeStruct((32, 256), BF16), pltpu.VMEM(state.shape, F32)),
+        in_specs=[hbm, vmem, vmem] + [hbm] * 7 + [vmem] * 3 + [hbm],
+        out_specs=(vmem, vmem),
         scratch_shapes=[
             pltpu.VMEM((4, 4, 4, 4, 4, 16, 128), BF16),
             pltpu.VMEM((2, 384, 4096), BF16),
             pltpu.VMEM((2, 64, 4096), BF16),
-            pltpu.VMEM((2, 32, 4, 64, 64), F32),
             pltpu.VMEM((2, 4, 32, 384), BF16),
             pltpu.VMEM((2, 4, 32, 384), BF16),
             pltpu.VMEM((4, 32, 128), BF16),
             pltpu.VMEM((4, 32, 128), BF16),
             pltpu.VMEM((256, 128), F32),
             pltpu.VMEM((2, 256, 128), F32),
+            pltpu.VMEM((32, 256), F32),
+            pltpu.VMEM((32, 256), F32),
+            pltpu.VMEM((256, 128), F32),
+            pltpu.VMEM((256, 128), F32),
             pltpu.SemaphoreType.DMA((4, 4, 3)),
             pltpu.SemaphoreType.DMA((4, 4, 5)),
             pltpu.SemaphoreType.DMA((3,)),
@@ -377,23 +389,9 @@
             pltpu.SemaphoreType.DMA((2,)),
             pltpu.SemaphoreType.DMA((4,)),
         ],
-        compiler_params=pltpu.CompilerParams(collective_id=0, has_side_effects=True),
+        compiler_params=pltpu.CompilerParams(collective_id=0, has_side_effects=True, vmem_limit_bytes=52 << 20),
         name="decode_step",
     )(tokens, lengths.reshape(1, 32), norm_gain, *weights, decay_base, rate_base, group_gain, state)
-    new_state = pl.pallas_call(
-        update_kernel,
-        grid=(2, 4),
-        out_shape=jax.ShapeDtypeStruct(state.shape, F32),
-        in_specs=[
-            pl.BlockSpec((1, 8, 4, 64, 64), lambda l, i: (l, i, 0, 0, 0)),
-            pl.BlockSpec((1, 8, 256), lambda l, i: (l, i, 0)),
-            pl.BlockSpec((1, 8, 256), lambda l, i: (l, i, 0)),
-            pl.BlockSpec((1, 64, 128), lambda l, i: (l, i, 0)),
-            pl.BlockSpec((1, 64, 128), lambda l, i: (l, i, 0)),
-        ],
-        out_specs=pl.BlockSpec((1, 8, 4, 64, 64), lambda l, i: (l, i, 0, 0, 0)),
-        name="state_update",
-    )(state, sa, val, pq, dec)
     return mixed, new_state
 
 

time: 90.8 us -> 83.6 us (0.921)
  Pallas kernels: 89.1 us -> 78.8 us
  local copies, waits for them, and re-layouts: 0.61 us -> 4.01 us
    pallas_call x1 -> x0, Pallas kernels: 10.2 us -> none  [local(): pl.pallas_call(update_kernel, grid=(2, 4), out_shape=jax.ShapeDtypeStruct...]
    unnamed x3 -> x4, local copies, waits for them, and re-layouts: 0.61 us -> 4.01 us
where the time goes in v2:
time: 83.6 us; the launch traced here: 83.4 us
  Pallas kernels  78.8 us (94%)
  local copies, waits for them, and re-layouts  4.01 us (5%)
    pallas_call x1, Pallas kernels, local(): pl.pallas_call(step_kernel, out_shape=(jax.ShapeDtypeStruct((32, 256), BF...  78.8 us
    unnamed x4, local copies, waits for them, and re-layouts  4.01 us

profile of v2, /device:TPU:0, one launch (start us, length us, event | category | flops | bytes accessed | tf_op | source)
XLA Modules:
  0.0 83.4 jit_solution(12526364179076657397)
XLA Ops:
  0.6 78.8 %decode_step.1 = (bf16[32,256]{1,0:T(8,128)(2,1)}, f32[2,32,4,64,64]{4,3,2,1,0:T(8,128)S(1)}) custom-call(bf16[32,256]{1,0:T(8,128)(2,1)} %tok.1, s32[1,32]{1,0:T(1,128)} %bitcast.15, f32[2,4096]{1,0:T(2,128)} %gain.1, bf16[2,32,4096]{2,1,0:T(8,128)(2,1)} %bitcast.8, bf16[2,32,4096]{2,1,0:T(8,128)(2,1)} %bitcast.9, bf16[2,32,4096]{2,1,0:T(8,128)(2,1)} %bitcast.10, ...), custom_call_target="tpu_custom_call" | custom-call | tf_op jit(solution)/shard_map/decode_step/pallas_call | solution.py:363
  79.4 0.0 copy-start
  79.4 3.4 %copy.18 = f32[2,32,4,64,64]{4,3,2,1,0:T(8,128)} copy(f32[2,32,4,64,64]{4,3,2,1,0:T(8,128)S(1)} %get-tuple-element.3) | data formatting | bytes 8388608
  82.8 0.0 copy-done
  82.8 0.6 copy.19
Async XLA Ops:
  79.4 3.4 %copy-start = (bf16[32,256]{1,0:T(8,128)(2,1)S(1)}, bf16[32,256]{1,0:T(8,128)(2,1)}, u32[]{:S(2)}) copy-start(bf16[32,256]{1,0:T(8,128)(2,1)} %get-tuple-element.6) | copy-start | bytes 49156

commit v3 on v2

--- a/solution.py
+++ b/solution.py
@@ -20,27 +20,30 @@
 
 
 def step_kernel(
-    tok, lens, gain, w0, w1, w2, w3, w4, w5, w_out, dbase, rbase, ggain, state,
+    tok, lens_in, gain_in, w0, w1, w2, w3, w4, w5, w_out, dbase_in, rbase_in, ggain_in, state,
     mixed, ST,
-    G, WP, WO, SB, RB, FB, FR, V8, M2, SA, VA, PQ, DEC,
-    g_send, g_recv, a_send, a_recv, w_local, w_send, w_recv, st_sem, tok_sem,
+    G, WP, WO, SB, RB, FB, FR, V8, M2, SA, VA, PQ, DEC, lens, gain, dbase, rbase, ggain,
+    g_send, g_recv, a_send, a_recv, w_local, w_send, w_recv, st_sem, tok_sem, small_sem,
 ):
     tp, dp = lax.axis_index("tp"), lax.axis_index("dp")
     c = dp % 2
     at = {"z": tp // 4, "y": tp % 4, "x": dp // 2}
     projections = (w0, w1, w2, w3, w4, w5)
 
-    def device(axis, hop):
-        to = dict(at)
-        to[axis] = (at[axis] + hop) % 4
+    def device(**hops):
+        to = {axis: (at[axis] + hops.get(axis, 0)) % 4 for axis in "xyz"}
         return (to["z"] * 4 + to["y"], to["x"] * 2 + c)
 
     partner = (tp, at["x"] * 2 + 1 - c)
 
     barrier = pltpu.get_barrier_semaphore()
-    for axis in "xyz":
-        for hop in (1, 2, 3):
-            pl.semaphore_signal(barrier, inc=1, device_id=device(axis, hop), device_id_type=MESH)
+    peers = [
+        dict(x=hx, y=hy, z=hz) for hx in range(4) for hy in range(4) for hz in range(4)
+        if 0 in (hx, hy, hz) and (hx, hy, hz) != (0, 0, 0)
+    ]
+    for peer in peers:
+        pl.semaphore_signal(barrier, inc=1, device_id=device(**peer), device_id_type=MESH)
+    pl.semaphore_signal(barrier, inc=1, device_id=partner, device_id_type=MESH)
 
     tok_copies = []
     for q in range(4):
@@ -52,7 +55,8 @@
         ))
         tok_copies[-1].start()
     mine = pl.multiple_of(c * 32, 32)
-    for layer in range(2):
+
+    def weights_local(layer):
         for kind in range(6):
             pltpu.make_async_copy(
                 projections[kind].at[layer],
@@ -63,18 +67,25 @@
             w_out.at[layer], WO.at[layer, pl.ds(mine, 32)], w_local.at[layer, 1]
         ).start()
 
-    pl.semaphore_wait(barrier, 9 + c)
-    pl.semaphore_signal(barrier, inc=1, device_id=partner, device_id_type=MESH)
+    small = [
+        pltpu.make_async_copy(src, dst, small_sem.at[i])
+        for i, (src, dst) in enumerate(
+            ((lens_in, lens), (gain_in, gain), (dbase_in, dbase), (rbase_in, rbase), (ggain_in, ggain)))
+    ]
+    for copy in small:
+        copy.start()
+    weights_local(0)
+    pl.semaphore_wait(barrier, len(peers) + 1)
 
     def block(a, q, free, moved=None):
         idx = [moved[ax] if moved and ax in moved else at[ax] for ax in "zyx"]
         idx = [slice(None) if ax in free else i for ax, i in zip("zyx", idx)]
         return G.at[(a, q, *idx)]
 
-    def send(ref, axis, hop, send_sem, recv_sem):
+    def send(ref, send_sem, recv_sem, **hops):
         pltpu.make_async_remote_copy(
             src_ref=ref, dst_ref=ref, send_sem=send_sem, recv_sem=recv_sem,
-            device_id=device(axis, hop), device_id_type=MESH,
+            device_id=device(**hops), device_id_type=MESH,
         ).start()
 
     def landed(ref, sem):
@@ -82,26 +93,29 @@
 
     def gather_first(a):
         for q in range(4):
+            first, second, third = ORDERS[q]
             if a == 0:
                 tok_copies[q].wait()
-            for hop in (1, 2, 3):
-                send(block(a, q, ()), ORDERS[q][0], hop, g_send.at[a, q, 0], g_recv.at[a, q, 0])
+            for hop in (2, 1, 3):
+                send(block(a, q, ()), g_send.at[a, q, 0], g_recv.at[a, q, 0], **{first: hop})
+            for over in (2, 1, 3):
+                for hop in (2, 1, 3, 0):
+                    send(block(a, q, ()), g_send.at[a, q, 1], g_recv.at[a, q, over],
+                         **{first: hop, second: over})
 
     def gather_middle(a):
         for q in range(4):
             first, second, third = ORDERS[q]
             landed(G.at[a, q, 0, 0, pl.ds(0, 3)], g_recv.at[a, q, 0])
-            for hop in (2, 1, 3):
-                send(block(a, q, first), second, hop, g_send.at[a, q, 1], g_recv.at[a, q, hop])
-            for hop in (2, 1, 3):
-                send(block(a, q, first), third, hop, g_send.at[a, q, 2], g_recv.at[a, q, 4])
-        for hop in (1, 3, 2):
+            for on in (2, 1, 3):
+                send(block(a, q, first), g_send.at[a, q, 2], g_recv.at[a, q, 4], **{third: on})
+        for over in (1, 3, 2):
             for q in range(4):
                 first, second, third = ORDERS[q]
-                landed(G.at[a, q, 0, 0], g_recv.at[a, q, hop])
-                line = {second: (at[second] + 4 - hop) % 4}
+                landed(G.at[a, q, 0, 0], g_recv.at[a, q, over])
+                line = {second: (at[second] + 4 - over) % 4}
                 for on in (2, 1, 3):
-                    send(block(a, q, first, line), third, on, g_send.at[a, q, 2], g_recv.at[a, q, 4])
+                    send(block(a, q, first, line), g_send.at[a, q, 2], g_recv.at[a, q, 4], **{third: on})
 
     def gather_last(a):
         for q in range(4):
@@ -121,41 +135,42 @@
                 parts.append(jnp.concatenate(halves, axis=0))
         return parts
 
-    def exchange(n, src, dst):
+    def exchange_start(n, src, dst):
         for hop in (2, 1, 3):
             to = (at["x"] + hop) % 4
             pltpu.make_async_remote_copy(
                 src_ref=src.at[to], dst_ref=dst.at[at["x"]],
                 send_sem=a_send.at[n], recv_sem=a_recv.at[n],
-                device_id=device("x", hop), device_id_type=MESH,
+                device_id=device(x=hop), device_id_type=MESH,
             ).start()
         dst[at["x"]] = src[at["x"]]
+
+    def exchange_done(n, dst):
         landed(dst.at[pl.ds(0, 3)], a_recv.at[n])
 
     def exchange_sent(n, src):
         landed(src.at[pl.ds(0, 3)], a_send.at[n])
 
-    def weights_out():
-        for layer in range(2):
-            for kind in range(6):
-                pltpu.make_async_remote_copy(
-                    src_ref=projections[kind].at[layer],
-                    dst_ref=WP.at[layer, pl.ds(kind * 64 + mine, 32)],
-                    send_sem=w_send.at[layer, 0], recv_sem=w_recv.at[layer, 0],
-                    device_id=partner, device_id_type=MESH,
-                ).start()
+    def projections_out(layer):
+        for kind in range(6):
             pltpu.make_async_remote_copy(
-                src_ref=w_out.at[layer],
-                dst_ref=WO.at[layer, pl.ds(mine, 32)],
-                send_sem=w_send.at[layer, 1], recv_sem=w_recv.at[layer, 1],
+                src_ref=projections[kind].at[layer],
+                dst_ref=WP.at[layer, pl.ds(kind * 64 + mine, 32)],
+                send_sem=w_send.at[layer, 0], recv_sem=w_recv.at[layer, 0],
                 device_id=partner, device_id_type=MESH,
             ).start()
 
-    def weights_in(layer):
+    def output_out(layer):
+        pltpu.make_async_remote_copy(
+            src_ref=w_out.at[layer],
+            dst_ref=WO.at[layer, pl.ds(mine, 32)],
+            send_sem=w_send.at[layer, 1], recv_sem=w_recv.at[layer, 1],
+            device_id=partner, device_id_type=MESH,
+        ).start()
+
+    def projections_in(layer):
         landed(WP.at[layer, pl.ds(0, 192)], w_local.at[layer, 0])
         landed(WP.at[layer, pl.ds(0, 192)], w_recv.at[layer, 0])
-        landed(WO.at[layer, pl.ds(0, 32)], w_local.at[layer, 1])
-        landed(WO.at[layer, pl.ds(0, 32)], w_recv.at[layer, 1])
         scale = gain[layer:layer + 1, :]
 
         def fold(i, carry):
@@ -164,6 +179,10 @@
             return carry
 
         lax.fori_loop(0, 24, fold, 0)
+
+    def output_in(layer):
+        landed(WO.at[layer, pl.ds(0, 32)], w_local.at[layer, 1])
+        landed(WO.at[layer, pl.ds(0, 32)], w_recv.at[layer, 1])
 
     def weights_sent():
         for layer in range(2):
@@ -206,14 +225,17 @@
         factor = lax.rsqrt(jnp.sum(squares, axis=0, keepdims=True) * (1.0 / 4096) + RMS_EPS)
         put_projected(1, (acc * factor).T)
 
-    ident = lax.broadcasted_iota(jnp.int32, (32, 32), 0) == lax.broadcasted_iota(jnp.int32, (32, 32), 1)
-    length = jnp.sum(jnp.where(ident, jnp.broadcast_to(lens[0:1, :], (32, 32)), 0), axis=1, keepdims=True)
-    active = length > STEP
+    def active_rows():
+        row = lax.broadcasted_iota(jnp.int32, (32, 32), 0)
+        col = lax.broadcasted_iota(jnp.int32, (32, 32), 1)
+        spread = jnp.broadcast_to(lens[0:1, :], (32, 32))
+        return jnp.sum(jnp.where(row == col, spread, 0), axis=1, keepdims=True) > STEP
 
     def wide128(value):
         return jnp.concatenate([value, jnp.zeros_like(value)], axis=1)
 
     def recur(layer, a):
+        active = active_rows()
         values, gates, first_sums, second_sums = [], [], [], []
         for h in range(4):
             take = lambda kind: RB[layer, h, :, kind * 64:(kind + 1) * 64].astype(F32)
@@ -283,70 +305,71 @@
                 ST[layer, b, h] = (ST[layer, b, h] * DEC[b * 8 + h:b * 8 + h + 1, 0:64]
                                    + delta[h * 64:(h + 1) * 64, :])
 
+    def output_first():
+        acc = jnp.zeros((64, 128), F32)
+        for z in range(4):
+            acc += lax.dot_general(
+                WO[0, :, z * 1024:(z + 1) * 1024], jnp.concatenate(rows_chunk(1, z), axis=1), LANES,
+                preferred_element_type=F32,
+            )
+        out = acc.astype(BF16)
+        for q in range(4):
+            G[2, q, at["z"], at["y"], at["x"]] = out[q * 16:(q + 1) * 16, :]
+
+    def output_second():
+        acc = jnp.zeros((128, 64), F32)
+        for z in range(4):
+            acc += lax.dot_general(
+                jnp.concatenate(rows_chunk(3, z), axis=1), WO[1, :, z * 1024:(z + 1) * 1024], LANES,
+                preferred_element_type=F32,
+            )
+        out = wide128(acc).astype(BF16)
+        for to in range(4):
+            FB[to, 0:16, :] = out[to * 16:to * 16 + 16, :]
+            FB[to, 16:32, :] = out[64 + to * 16:64 + to * 16 + 16, :]
+
     gather_first(0)
-    for layer in range(2):
-        pltpu.make_async_copy(state.at[layer], ST.at[layer], st_sem.at[layer]).start()
-
-    @pl.when(c == 1)
-    def _():
-        weights_out()
-
+    projections_out(0)
+    pltpu.make_async_copy(state.at[0], ST.at[0], st_sem.at[0]).start()
+    weights_local(1)
+    pltpu.make_async_copy(state.at[1], ST.at[1], st_sem.at[1]).start()
     gather_middle(0)
-
-    @pl.when(c == 0)
-    def _():
-        pl.semaphore_wait(barrier, 1)
-        weights_out()
-
-    weights_in(0)
+    for copy in small:
+        copy.wait()
+    projections_in(0)
     gather_last(0)
     project_first()
-    exchange(0, SB.at[0], RB.at[0])
+    exchange_start(0, SB.at[0], RB.at[0])
+    output_out(0)
+    projections_out(1)
+    output_out(1)
+    exchange_done(0, RB.at[0])
     landed(ST.at[0], st_sem.at[0])
     recur(0, 1)
-
     gather_first(1)
-    update(0, 0, 10)
+    update(0, 0, 32)
     gather_middle(1)
-    update(0, 10, 22)
-    weights_in(1)
+    projections_in(1)
+    output_in(0)
+    output_in(1)
     gather_last(1)
-    acc = jnp.zeros((64, 128), F32)
-    for z in range(4):
-        acc += lax.dot_general(
-            WO[0, :, z * 1024:(z + 1) * 1024], jnp.concatenate(rows_chunk(1, z), axis=1), LANES,
-            preferred_element_type=F32,
-        )
-    out = acc.astype(BF16)
-    for q in range(4):
-        G[2, q, at["z"], at["y"], at["x"]] = out[q * 16:(q + 1) * 16, :]
-
+    output_first()
     gather_first(2)
     gather_middle(2)
     gather_last(2)
     project_second()
-    exchange(1, SB.at[1], RB.at[1])
+    exchange_start(1, SB.at[1], RB.at[1])
+    exchange_done(1, RB.at[1])
     landed(ST.at[1], st_sem.at[1])
     recur(1, 3)
-
     gather_first(3)
-    update(1, 0, 10)
+    update(1, 0, 32)
     gather_middle(3)
-    update(1, 10, 22)
     gather_last(3)
-    acc = jnp.zeros((128, 64), F32)
-    for z in range(4):
-        acc += lax.dot_general(
-            jnp.concatenate(rows_chunk(3, z), axis=1), WO[1, :, z * 1024:(z + 1) * 1024], LANES,
-            preferred_element_type=F32,
-        )
-    out = wide128(acc).astype(BF16)
-    for to in range(4):
-        FB[to, 0:16, :] = out[to * 16:to * 16 + 16, :]
-        FB[to, 16:32, :] = out[64 + to * 16:64 + to * 16 + 16, :]
-    exchange(2, FB, FR)
+    output_second()
+    exchange_start(2, FB, FR)
+    exchange_done(2, FR)
     mixed[...] = jnp.concatenate([FR[h, :, 0:64] for h in range(4)], axis=1)
-
     for a in range(4):
         gather_sent(a)
     exchange_sent(0, SB.at[0])
@@ -363,7 +386,7 @@
     mixed, new_state = pl.pallas_call(
         step_kernel,
         out_shape=(jax.ShapeDtypeStruct((32, 256), BF16), pltpu.VMEM(state.shape, F32)),
-        in_specs=[hbm, vmem, vmem] + [hbm] * 7 + [vmem] * 3 + [hbm],
+        in_specs=[hbm] * 14,
         out_specs=(vmem, vmem),
         scratch_shapes=[
             pltpu.VMEM((4, 4, 4, 4, 4, 16, 128), BF16),
@@ -379,6 +402,11 @@
             pltpu.VMEM((32, 256), F32),
             pltpu.VMEM((256, 128), F32),
             pltpu.VMEM((256, 128), F32),
+            pltpu.VMEM((1, 32), jnp.int32),
+            pltpu.VMEM((2, 4096), F32),
+            pltpu.VMEM((2, 256), F32),
+            pltpu.VMEM((2, 256), F32),
+            pltpu.VMEM((2, 256), F32),
             pltpu.SemaphoreType.DMA((4, 4, 3)),
             pltpu.SemaphoreType.DMA((4, 4, 5)),
             pltpu.SemaphoreType.DMA((3,)),
@@ -388,6 +416,7 @@
             pltpu.SemaphoreType.DMA((2, 2)),
             pltpu.SemaphoreType.DMA((2,)),
             pltpu.SemaphoreType.DMA((4,)),
+            pltpu.SemaphoreType.DMA((5,)),
         ],
         compiler_params=pltpu.CompilerParams(collective_id=0, has_side_effects=True, vmem_limit_bytes=52 << 20),
         name="decode_step",

time: 83.6 us -> 75.2 us (0.90)
  Pallas kernels: 78.8 us -> 70.5 us
    pallas_call x1, Pallas kernels: 78.8 us -> 70.5 us  [local(): pl.pallas_call(step_kernel, out_shape=(jax.ShapeDtypeStruct((32, 256), BF...]
where the time goes in v3:
time: 75.2 us; the launch traced here: 75.1 us
  Pallas kernels  70.5 us (94%)
  local copies, waits for them, and re-layouts  4.01 us (5%)
    pallas_call x1, Pallas kernels, local(): pl.pallas_call(step_kernel, out_shape=(jax.ShapeDtypeStruct((32, 256), BF...  70.5 us
    unnamed x4, local copies, waits for them, and re-layouts  4.01 us

profile of v3, /device:TPU:0, one launch (start us, length us, event | category | flops | bytes accessed | tf_op | source)
XLA Modules:
  0.0 75.1 jit_solution(11628178481947691484)
XLA Ops:
  0.6 70.5 %decode_step.1 = (bf16[32,256]{1,0:T(8,128)(2,1)}, f32[2,32,4,64,64]{4,3,2,1,0:T(8,128)S(1)}) custom-call(bf16[32,256]{1,0:T(8,128)(2,1)} %tok.1, s32[1,32]{1,0:T(1,128)} %bitcast.15, f32[2,4096]{1,0:T(2,128)} %gain_in.1, bf16[2,32,4096]{2,1,0:T(8,128)(2,1)} %bitcast.8, bf16[2,32,4096]{2,1,0:T(8,128)(2,1)} %bitcast.9, bf16[2,32,4096]{2,1,0:T(8,128)(2,1)} %bitcast.10, ...), custom_call_target="tpu_custom_call" | custom-call | tf_op jit(solution)/shard_map/decode_step/pallas_call | solution.py:386
  71.1 0.0 copy-start
  71.1 3.4 %copy.18 = f32[2,32,4,64,64]{4,3,2,1,0:T(8,128)} copy(f32[2,32,4,64,64]{4,3,2,1,0:T(8,128)S(1)} %get-tuple-element.3) | data formatting | bytes 8388608
  74.5 0.0 copy-done
  74.5 0.6 copy.19
Async XLA Ops:
  71.1 3.4 %copy-start = (bf16[32,256]{1,0:T(8,128)(2,1)S(1)}, bf16[32,256]{1,0:T(8,128)(2,1)}, u32[]{:S(2)}) copy-start(bf16[32,256]{1,0:T(8,128)(2,1)} %get-tuple-element.6) | copy-start | bytes 49156

commit v4 on v3

--- a/solution.py
+++ b/solution.py
@@ -13,17 +13,16 @@
 MESH = pl.DeviceIdType.MESH
 F32 = jnp.float32
 BF16 = jnp.bfloat16
-ORDERS = (("x", "y", "z"), ("y", "z", "x"), ("z", "x", "y"), ("y", "x", "z"))
+ORDERS = (("x", "y", "z"), ("x", "z", "y"), ("x", "y", "z"), ("x", "z", "y"))
 LANES = (((1,), (1,)), ((), ()))
-PLAIN = (((1,), (0,)), ((), ()))
 ROWS = (((0,), (0,)), ((), ()))
 
 
 def step_kernel(
     tok, lens_in, gain_in, w0, w1, w2, w3, w4, w5, w_out, dbase_in, rbase_in, ggain_in, state,
     mixed, ST,
-    G, WP, WO, SB, RB, FB, FR, V8, M2, SA, VA, PQ, DEC, lens, gain, dbase, rbase, ggain,
-    g_send, g_recv, a_send, a_recv, w_local, w_send, w_recv, st_sem, tok_sem, small_sem,
+    G, GP, WP, WO, SB, RB, V8, M2, SA, VA, PQ, DEC, lens, gain, dbase, rbase, ggain,
+    g_send, g_recv, p_send, p_recv, a_send, a_recv, w_local, w_send, w_recv, o_sem, st_sem, tok_sem, small_sem,
 ):
     tp, dp = lax.axis_index("tp"), lax.axis_index("dp")
     c = dp % 2
@@ -55,17 +54,16 @@
         ))
         tok_copies[-1].start()
     mine = pl.multiple_of(c * 32, 32)
+    own_cols = pl.multiple_of(dp * 32, 32)
 
     def weights_local(layer):
         for kind in range(6):
             pltpu.make_async_copy(
                 projections[kind].at[layer],
                 WP.at[layer, pl.ds(kind * 64 + mine, 32)],
-                w_local.at[layer, 0],
+                w_local.at[layer],
             ).start()
-        pltpu.make_async_copy(
-            w_out.at[layer], WO.at[layer, pl.ds(mine, 32)], w_local.at[layer, 1]
-        ).start()
+        pltpu.make_async_copy(w_out.at[layer], WO.at[layer, pl.ds(own_cols, 32)], o_sem.at[layer, 0]).start()
 
     small = [
         pltpu.make_async_copy(src, dst, small_sem.at[i])
@@ -156,21 +154,50 @@
             pltpu.make_async_remote_copy(
                 src_ref=projections[kind].at[layer],
                 dst_ref=WP.at[layer, pl.ds(kind * 64 + mine, 32)],
-                send_sem=w_send.at[layer, 0], recv_sem=w_recv.at[layer, 0],
+                send_sem=w_send.at[layer], recv_sem=w_recv.at[layer],
                 device_id=partner, device_id_type=MESH,
             ).start()
 
-    def output_out(layer):
+    def output_over_x(layer):
+        for part in range(4):
+            for hop in (2, 1, 3):
+                pltpu.make_async_remote_copy(
+                    src_ref=w_out.at[layer, pl.ds(part * 8, 8)],
+                    dst_ref=WO.at[layer, pl.ds(pl.multiple_of(own_cols + part * 8, 8), 8)],
+                    send_sem=o_sem.at[layer, 1], recv_sem=o_sem.at[layer, 2],
+                    device_id=device(x=hop), device_id_type=MESH,
+                ).start()
+
+    def output_to_partner(layer):
         pltpu.make_async_remote_copy(
-            src_ref=w_out.at[layer],
-            dst_ref=WO.at[layer, pl.ds(mine, 32)],
-            send_sem=w_send.at[layer, 1], recv_sem=w_recv.at[layer, 1],
+            src_ref=w_out.at[layer], dst_ref=WO.at[layer, pl.ds(own_cols, 32)],
+            send_sem=o_sem.at[layer, 3], recv_sem=o_sem.at[layer, 4],
             device_id=partner, device_id_type=MESH,
         ).start()
 
+    def output_pass_on(layer):
+        landed(WO.at[layer, pl.ds(0, 96)], o_sem.at[layer, 2])
+        for hop in (1, 2, 3):
+            cols = pl.ds(pl.multiple_of(((at["x"] + hop) % 4) * 64 + c * 32, 32), 32)
+            pltpu.make_async_remote_copy(
+                src_ref=WO.at[layer, cols], dst_ref=WO.at[layer, cols],
+                send_sem=o_sem.at[layer, 5], recv_sem=o_sem.at[layer, 6],
+                device_id=partner, device_id_type=MESH,
+            ).start()
+
+    def output_in(layer):
+        landed(WO.at[layer, pl.ds(0, 32)], o_sem.at[layer, 0])
+        landed(WO.at[layer, pl.ds(0, 32)], o_sem.at[layer, 4])
+        landed(WO.at[layer, pl.ds(0, 96)], o_sem.at[layer, 6])
+
+    def output_sent(layer):
+        landed(WO.at[layer, pl.ds(0, 96)], o_sem.at[layer, 1])
+        landed(WO.at[layer, pl.ds(0, 32)], o_sem.at[layer, 3])
+        landed(WO.at[layer, pl.ds(0, 96)], o_sem.at[layer, 5])
+
     def projections_in(layer):
-        landed(WP.at[layer, pl.ds(0, 192)], w_local.at[layer, 0])
-        landed(WP.at[layer, pl.ds(0, 192)], w_recv.at[layer, 0])
+        landed(WP.at[layer, pl.ds(0, 192)], w_local.at[layer])
+        landed(WP.at[layer, pl.ds(0, 192)], w_recv.at[layer])
         scale = gain[layer:layer + 1, :]
 
         def fold(i, carry):
@@ -180,14 +207,10 @@
 
         lax.fori_loop(0, 24, fold, 0)
 
-    def output_in(layer):
-        landed(WO.at[layer, pl.ds(0, 32)], w_local.at[layer, 1])
-        landed(WO.at[layer, pl.ds(0, 32)], w_recv.at[layer, 1])
-
     def weights_sent():
         for layer in range(2):
-            landed(WP.at[layer, pl.ds(0, 192)], w_send.at[layer, 0])
-            landed(WO.at[layer, pl.ds(0, 32)], w_send.at[layer, 1])
+            landed(WP.at[layer, pl.ds(0, 192)], w_send.at[layer])
+            output_sent(layer)
 
     def put_projected(layer, projected):
         out = projected.astype(BF16)
@@ -195,35 +218,20 @@
             SB[layer, to, 0:16, :] = out[to * 16:to * 16 + 16, :]
             SB[layer, to, 16:32, :] = out[64 + to * 16:64 + to * 16 + 16, :]
 
-    def project_first():
+    def project(layer):
         acc = jnp.zeros((128, 384), F32)
         squares = jnp.zeros((128, 128), F32)
         for z in range(4):
-            parts = rows_chunk(0, z)
+            parts = rows_chunk(layer, z)
             for part in parts:
                 wide = part.astype(F32)
                 squares += wide * wide
             acc += lax.dot_general(
-                jnp.concatenate(parts, axis=1), WP[0, :, z * 1024:(z + 1) * 1024], LANES,
+                jnp.concatenate(parts, axis=1), WP[layer, :, z * 1024:(z + 1) * 1024], LANES,
                 preferred_element_type=F32,
             )
         factor = lax.rsqrt(jnp.sum(squares, axis=1, keepdims=True) * (1.0 / 4096) + RMS_EPS)
-        put_projected(0, acc * factor)
-
-    def project_second():
-        acc = jnp.zeros((384, 128), F32)
-        squares = jnp.zeros((16, 128), F32)
-        for z in range(4):
-            parts = [G[2, q, z, y, x] for y in range(4) for x in range(4) for q in range(4)]
-            for part in parts:
-                wide = part.astype(F32)
-                squares += wide * wide
-            acc += lax.dot_general(
-                WP[1, :, z * 1024:(z + 1) * 1024], jnp.concatenate(parts, axis=0), PLAIN,
-                preferred_element_type=F32,
-            )
-        factor = lax.rsqrt(jnp.sum(squares, axis=0, keepdims=True) * (1.0 / 4096) + RMS_EPS)
-        put_projected(1, (acc * factor).T)
+        put_projected(layer, acc * factor)
 
     def active_rows():
         row = lax.broadcasted_iota(jnp.int32, (32, 32), 0)
@@ -234,7 +242,7 @@
     def wide128(value):
         return jnp.concatenate([value, jnp.zeros_like(value)], axis=1)
 
-    def recur(layer, a):
+    def recur(layer):
         active = active_rows()
         values, gates, first_sums, second_sums = [], [], [], []
         for h in range(4):
@@ -287,7 +295,7 @@
         rows = jnp.where(active, rows, 0.0).astype(BF16)
         for q in range(4):
             rh, ch = q // 2, q % 2
-            G[a, q, at["z"], at["y"], at["x"]] = rows[rh * 16:(rh + 1) * 16, ch * 128:(ch + 1) * 128]
+            GP[layer, tp, q] = rows[rh * 16:(rh + 1) * 16, ch * 128:(ch + 1) * 128]
 
     head_of = lax.broadcasted_iota(jnp.int32, (8, 256), 1) // 64
     row_of = lax.broadcasted_iota(jnp.int32, (8, 256), 0)
@@ -305,32 +313,33 @@
                 ST[layer, b, h] = (ST[layer, b, h] * DEC[b * 8 + h:b * 8 + h + 1, 0:64]
                                    + delta[h * 64:(h + 1) * 64, :])
 
-    def output_first():
-        acc = jnp.zeros((64, 128), F32)
+    def plane_first(layer):
+        here = GP.at[layer, tp]
+        for hop_z in (2, 1, 3, 0):
+            for hop_y in (2, 1, 3, 0):
+                if hop_z or hop_y:
+                    send(here, p_send.at[layer], p_recv.at[layer], z=hop_z, y=hop_y)
+
+    def plane_last(layer):
+        landed(GP.at[layer, pl.ds(0, 15)], p_recv.at[layer])
+
+    def output(layer):
+        acc = jnp.zeros((32, 256), F32)
         for z in range(4):
+            parts = [
+                jnp.concatenate([GP[layer, z * 4 + y, ch], GP[layer, z * 4 + y, 2 + ch]], axis=0)
+                for y in range(4) for ch in range(2)
+            ]
             acc += lax.dot_general(
-                WO[0, :, z * 1024:(z + 1) * 1024], jnp.concatenate(rows_chunk(1, z), axis=1), LANES,
+                jnp.concatenate(parts, axis=1), WO[layer, :, z * 1024:(z + 1) * 1024], LANES,
                 preferred_element_type=F32,
             )
-        out = acc.astype(BF16)
-        for q in range(4):
-            G[2, q, at["z"], at["y"], at["x"]] = out[q * 16:(q + 1) * 16, :]
-
-    def output_second():
-        acc = jnp.zeros((128, 64), F32)
-        for z in range(4):
-            acc += lax.dot_general(
-                jnp.concatenate(rows_chunk(3, z), axis=1), WO[1, :, z * 1024:(z + 1) * 1024], LANES,
-                preferred_element_type=F32,
-            )
-        out = wide128(acc).astype(BF16)
-        for to in range(4):
-            FB[to, 0:16, :] = out[to * 16:to * 16 + 16, :]
-            FB[to, 16:32, :] = out[64 + to * 16:64 + to * 16 + 16, :]
+        return acc.astype(BF16)
 
     gather_first(0)
     projections_out(0)
     pltpu.make_async_copy(state.at[0], ST.at[0], st_sem.at[0]).start()
+    output_over_x(0)
     weights_local(1)
     pltpu.make_async_copy(state.at[1], ST.at[1], st_sem.at[1]).start()
     gather_middle(0)
@@ -338,44 +347,56 @@
         copy.wait()
     projections_in(0)
     gather_last(0)
-    project_first()
+    project(0)
     exchange_start(0, SB.at[0], RB.at[0])
-    output_out(0)
+    output_to_partner(0)
     projections_out(1)
-    output_out(1)
+    output_to_partner(1)
     exchange_done(0, RB.at[0])
+    output_pass_on(0)
     landed(ST.at[0], st_sem.at[0])
-    recur(0, 1)
-    gather_first(1)
+    recur(0)
+    plane_first(0)
     update(0, 0, 32)
-    gather_middle(1)
     projections_in(1)
     output_in(0)
-    output_in(1)
+    plane_last(0)
+    out = output(0)
+    for q in range(4):
+        rh, ch = q // 2, q % 2
+        G[1, q, at["z"], at["y"], at["x"]] = out[rh * 16:(rh + 1) * 16, ch * 128:(ch + 1) * 128]
+    gather_first(1)
+    output_over_x(1)
+    gather_middle(1)
     gather_last(1)
-    output_first()
-    gather_first(2)
-    gather_middle(2)
-    gather_last(2)
-    project_second()
+    project(1)
     exchange_start(1, SB.at[1], RB.at[1])
     exchange_done(1, RB.at[1])
+    output_pass_on(1)
     landed(ST.at[1], st_sem.at[1])
-    recur(1, 3)
-    gather_first(3)
+    recur(1)
+    plane_first(1)
     update(1, 0, 32)
-    gather_middle(3)
-    gather_last(3)
-    output_second()
-    exchange_start(2, FB, FR)
-    exchange_done(2, FR)
-    mixed[...] = jnp.concatenate([FR[h, :, 0:64] for h in range(4)], axis=1)
-    for a in range(4):
+    output_in(1)
+    plane_last(1)
+    mixed[...] = output(1)
+    for a in range(2):
         gather_sent(a)
-    exchange_sent(0, SB.at[0])
-    exchange_sent(1, SB.at[1])
-    exchange_sent(2, FB)
+        exchange_sent(a, SB.at[a])
+        landed(GP.at[a, pl.ds(0, 15)], p_send.at[a])
     weights_sent()
+
+
+def finish_kernel(state_in, mixed_in, state_out, mixed_out, sem):
+    copies = [
+        pltpu.make_async_copy(state_in.at[0], state_out.at[0], sem.at[0]),
+        pltpu.make_async_copy(state_in.at[1], state_out.at[1], sem.at[1]),
+        pltpu.make_async_copy(mixed_in, mixed_out, sem.at[2]),
+    ]
+    for copy in copies:
+        copy.start()
+    for copy in copies:
+        copy.wait()
 
 
 def local(tokens, lengths, norm_gain, w_recept, w_key, w_value, w_decay, w_rate, w_gate, w_out,
@@ -383,19 +404,18 @@
     weights = [jnp.swapaxes(w, 1, 2) for w in (w_recept, w_key, w_value, w_decay, w_rate, w_gate, w_out)]
     hbm = pl.BlockSpec(memory_space=pltpu.HBM)
     vmem = pl.BlockSpec(memory_space=pltpu.VMEM)
-    mixed, new_state = pl.pallas_call(
+    mixed, stepped = pl.pallas_call(
         step_kernel,
-        out_shape=(jax.ShapeDtypeStruct((32, 256), BF16), pltpu.VMEM(state.shape, F32)),
+        out_shape=(pltpu.VMEM((32, 256), BF16), pltpu.VMEM(state.shape, F32)),
         in_specs=[hbm] * 14,
         out_specs=(vmem, vmem),
         scratch_shapes=[
-            pltpu.VMEM((4, 4, 4, 4, 4, 16, 128), BF16),
+            pltpu.VMEM((2, 4, 4, 4, 4, 16, 128), BF16),
+            pltpu.VMEM((2, 16, 4, 16, 128), BF16),
             pltpu.VMEM((2, 384, 4096), BF16),
-            pltpu.VMEM((2, 64, 4096), BF16),
+            pltpu.VMEM((2, 256, 4096), BF16),
             pltpu.VMEM((2, 4, 32, 384), BF16),
             pltpu.VMEM((2, 4, 32, 384), BF16),
-            pltpu.VMEM((4, 32, 128), BF16),
-            pltpu.VMEM((4, 32, 128), BF16),
             pltpu.VMEM((256, 128), F32),
             pltpu.VMEM((2, 256, 128), F32),
             pltpu.VMEM((32, 256), F32),
@@ -407,13 +427,16 @@
             pltpu.VMEM((2, 256), F32),
             pltpu.VMEM((2, 256), F32),
             pltpu.VMEM((2, 256), F32),
-            pltpu.SemaphoreType.DMA((4, 4, 3)),
-            pltpu.SemaphoreType.DMA((4, 4, 5)),
-            pltpu.SemaphoreType.DMA((3,)),
-            pltpu.SemaphoreType.DMA((3,)),
-            pltpu.SemaphoreType.DMA((2, 2)),
-            pltpu.SemaphoreType.DMA((2, 2)),
-            pltpu.SemaphoreType.DMA((2, 2)),
+            pltpu.SemaphoreType.DMA((2, 4, 3)),
+            pltpu.SemaphoreType.DMA((2, 4, 5)),
+            pltpu.SemaphoreType.DMA((2,)),
+            pltpu.SemaphoreType.DMA((2,)),
+            pltpu.SemaphoreType.DMA((2,)),
+            pltpu.SemaphoreType.DMA((2,)),
+            pltpu.SemaphoreType.DMA((2,)),
+            pltpu.SemaphoreType.DMA((2,)),
+            pltpu.SemaphoreType.DMA((2,)),
+            pltpu.SemaphoreType.DMA((2, 7)),
             pltpu.SemaphoreType.DMA((2,)),
             pltpu.SemaphoreType.DMA((4,)),
             pltpu.SemaphoreType.DMA((5,)),
@@ -421,6 +444,15 @@
         compiler_params=pltpu.CompilerParams(collective_id=0, has_side_effects=True, vmem_limit_bytes=52 << 20),
         name="decode_step",
     )(tokens, lengths.reshape(1, 32), norm_gain, *weights, decay_base, rate_base, group_gain, state)
+    new_state, mixed = pl.pallas_call(
+        finish_kernel,
+        out_shape=(pltpu.HBM(state.shape, F32), pltpu.HBM((32, 256), BF16)),
+        in_specs=[vmem, vmem],
+        out_specs=(hbm, hbm),
+        scratch_shapes=[pltpu.SemaphoreType.DMA((3,))],
+        compiler_params=pltpu.CompilerParams(vmem_limit_bytes=1 << 20),
+        name="finish",
+    )(stepped, mixed)
     return mixed, new_state
 
 

time: 75.2 us -> 63.2 us (0.84)
  Pallas kernels: 70.5 us -> 62.4 us
  local copies, waits for them, and re-layouts: 4.01 us -> 0 us
    pallas_call x1 -> x2, Pallas kernels: 70.5 us -> 62.4 us  [the longest x1 59 us: local(): pl.pallas_call(step_kernel, out_shape=(pltpu.VMEM((32, 256), BF16), pltpu...]
    unnamed x4 -> x0, local copies, waits for them, and re-layouts: 4.01 us -> none
where the time goes in v4:
time: 63.2 us; the launch traced here: 63.1 us
  Pallas kernels  62.4 us (99%)
  between operations  0.64 us (1%)
    pallas_call x1, Pallas kernels, local(): pl.pallas_call(step_kernel, out_shape=(pltpu.VMEM((32, 256), BF16), pltpu...  59 us
    pallas_call x1, Pallas kernels, local(): pl.pallas_call(finish_kernel, out_shape=(pltpu.HBM(state.shape, F32), plt...  3.42 us

profile of v4, /device:TPU:0, one launch (start us, length us, event | category | flops | bytes accessed | tf_op | source)
XLA Modules:
  0.0 63.1 jit_solution(1488032321412664486)
XLA Ops:
  0.6 59.0 %decode_step.1 = (bf16[32,256]{1,0:T(8,128)(2,1)S(1)}, f32[2,32,4,64,64]{4,3,2,1,0:T(8,128)S(1)}) custom-call(bf16[32,256]{1,0:T(8,128)(2,1)} %tok.1, s32[1,32]{1,0:T(1,128)} %bitcast.15, f32[2,4096]{1,0:T(2,128)} %gain_in.1, bf16[2,32,4096]{2,1,0:T(8,128)(2,1)} %bitcast.8, bf16[2,32,4096]{2,1,0:T(8,128)(2,1)} %bitcast.9, bf16[2,32,4096]{2,1,0:T(8,128)(2,1)} %bitcast.10, ...), custom_call_target="tpu_custom_call" | custom-call | tf_op jit(solution)/shard_map/decode_step/pallas_call | solution.py:407
  59.6 3.4 %finish.1 = (f32[2,32,4,64,64]{4,3,2,1,0:T(8,128)}, bf16[32,256]{1,0:T(8,128)(2,1)}) custom-call(f32[2,32,4,64,64]{4,3,2,1,0:T(8,128)S(1)} %get-tuple-element.6.state_in, bf16[32,256]{1,0:T(8,128)(2,1)S(1)} %get-tuple-element.7.mixed_in), custom_call_target="tpu_custom_call" | custom-call | tf_op jit(solution)/shard_map/finish/pallas_call | solution.py:447

commit v5 on v4

--- a/solution.py
+++ b/solution.py
@@ -18,16 +18,31 @@
 ROWS = (((0,), (0,)), ((), ()))
 
 
+def output_product(rows, weight):
+    acc = jnp.zeros((32, 256), F32)
+    for z in range(4):
+        parts = [
+            jnp.concatenate([rows[z * 4 + y, ch], rows[z * 4 + y, 2 + ch]], axis=0)
+            for y in range(4) for ch in range(2)
+        ]
+        acc += lax.dot_general(
+            jnp.concatenate(parts, axis=1), weight[:, z * 1024:(z + 1) * 1024], LANES,
+            preferred_element_type=F32,
+        )
+    return acc.astype(BF16)
+
+
 def step_kernel(
     tok, lens_in, gain_in, w0, w1, w2, w3, w4, w5, w_out, dbase_in, rbase_in, ggain_in, state,
-    mixed, ST,
-    G, GP, WP, WO, SB, RB, V8, M2, SA, VA, PQ, DEC, lens, gain, dbase, rbase, ggain,
+    ST, GP1, WO1,
+    G, GP0, WP, WO0, SA4, RA4, SB2, RB2, V8, M2, SA, VA, PQ, DEC, lens, gain, dbase, rbase, ggain,
     g_send, g_recv, p_send, p_recv, a_send, a_recv, w_local, w_send, w_recv, o_sem, st_sem, tok_sem, small_sem,
 ):
     tp, dp = lax.axis_index("tp"), lax.axis_index("dp")
     c = dp % 2
     at = {"z": tp // 4, "y": tp % 4, "x": dp // 2}
     projections = (w0, w1, w2, w3, w4, w5)
+    GP, WO = (GP0, GP1), (WO0, WO1)
 
     def device(**hops):
         to = {axis: (at[axis] + hops.get(axis, 0)) % 4 for axis in "xyz"}
@@ -63,7 +78,7 @@
                 WP.at[layer, pl.ds(kind * 64 + mine, 32)],
                 w_local.at[layer],
             ).start()
-        pltpu.make_async_copy(w_out.at[layer], WO.at[layer, pl.ds(own_cols, 32)], o_sem.at[layer, 0]).start()
+        pltpu.make_async_copy(w_out.at[layer], WO[layer].at[pl.ds(own_cols, 32)], o_sem.at[layer, 0]).start()
 
     small = [
         pltpu.make_async_copy(src, dst, small_sem.at[i])
@@ -163,37 +178,37 @@
             for hop in (2, 1, 3):
                 pltpu.make_async_remote_copy(
                     src_ref=w_out.at[layer, pl.ds(part * 8, 8)],
-                    dst_ref=WO.at[layer, pl.ds(pl.multiple_of(own_cols + part * 8, 8), 8)],
+                    dst_ref=WO[layer].at[pl.ds(pl.multiple_of(own_cols + part * 8, 8), 8)],
                     send_sem=o_sem.at[layer, 1], recv_sem=o_sem.at[layer, 2],
                     device_id=device(x=hop), device_id_type=MESH,
                 ).start()
 
     def output_to_partner(layer):
         pltpu.make_async_remote_copy(
-            src_ref=w_out.at[layer], dst_ref=WO.at[layer, pl.ds(own_cols, 32)],
+            src_ref=w_out.at[layer], dst_ref=WO[layer].at[pl.ds(own_cols, 32)],
             send_sem=o_sem.at[layer, 3], recv_sem=o_sem.at[layer, 4],
             device_id=partner, device_id_type=MESH,
         ).start()
 
     def output_pass_on(layer):
-        landed(WO.at[layer, pl.ds(0, 96)], o_sem.at[layer, 2])
+        landed(WO[layer].at[pl.ds(0, 96)], o_sem.at[layer, 2])
         for hop in (1, 2, 3):
             cols = pl.ds(pl.multiple_of(((at["x"] + hop) % 4) * 64 + c * 32, 32), 32)
             pltpu.make_async_remote_copy(
-                src_ref=WO.at[layer, cols], dst_ref=WO.at[layer, cols],
+                src_ref=WO[layer].at[cols], dst_ref=WO[layer].at[cols],
                 send_sem=o_sem.at[layer, 5], recv_sem=o_sem.at[layer, 6],
                 device_id=partner, device_id_type=MESH,
             ).start()
 
     def output_in(layer):
-        landed(WO.at[layer, pl.ds(0, 32)], o_sem.at[layer, 0])
-        landed(WO.at[layer, pl.ds(0, 32)], o_sem.at[layer, 4])
-        landed(WO.at[layer, pl.ds(0, 96)], o_sem.at[layer, 6])
+        landed(WO[layer].at[pl.ds(0, 32)], o_sem.at[layer, 0])
+        landed(WO[layer].at[pl.ds(0, 32)], o_sem.at[layer, 4])
+        landed(WO[layer].at[pl.ds(0, 96)], o_sem.at[layer, 6])
 
     def output_sent(layer):
-        landed(WO.at[layer, pl.ds(0, 96)], o_sem.at[layer, 1])
-        landed(WO.at[layer, pl.ds(0, 32)], o_sem.at[layer, 3])
-        landed(WO.at[layer, pl.ds(0, 96)], o_sem.at[layer, 5])
+        landed(WO[layer].at[pl.ds(0, 96)], o_sem.at[layer, 1])
+        landed(WO[layer].at[pl.ds(0, 32)], o_sem.at[layer, 3])
+        landed(WO[layer].at[pl.ds(0, 96)], o_sem.at[layer, 5])
 
     def projections_in(layer):
         landed(WP.at[layer, pl.ds(0, 192)], w_local.at[layer])
@@ -212,26 +227,35 @@
             landed(WP.at[layer, pl.ds(0, 192)], w_send.at[layer])
             output_sent(layer)
 
-    def put_projected(layer, projected):
+    def put_projected(projected, dst):
         out = projected.astype(BF16)
         for to in range(4):
-            SB[layer, to, 0:16, :] = out[to * 16:to * 16 + 16, :]
-            SB[layer, to, 16:32, :] = out[64 + to * 16:64 + to * 16 + 16, :]
+            dst[to, 0:16, :] = out[to * 16:to * 16 + 16, :]
+            dst[to, 16:32, :] = out[64 + to * 16:64 + to * 16 + 16, :]
 
     def project(layer):
-        acc = jnp.zeros((128, 384), F32)
         squares = jnp.zeros((128, 128), F32)
+        acc = jnp.zeros((128, 256), F32)
         for z in range(4):
             parts = rows_chunk(layer, z)
             for part in parts:
                 wide = part.astype(F32)
                 squares += wide * wide
             acc += lax.dot_general(
-                jnp.concatenate(parts, axis=1), WP[layer, :, z * 1024:(z + 1) * 1024], LANES,
+                jnp.concatenate(parts, axis=1), WP[layer, 0:256, z * 1024:(z + 1) * 1024], LANES,
                 preferred_element_type=F32,
             )
         factor = lax.rsqrt(jnp.sum(squares, axis=1, keepdims=True) * (1.0 / 4096) + RMS_EPS)
-        put_projected(layer, acc * factor)
+        put_projected(acc * factor, SA4.at[layer])
+        exchange_start(2 * layer, SA4.at[layer], RA4.at[layer])
+        acc = jnp.zeros((128, 128), F32)
+        for z in range(4):
+            acc += lax.dot_general(
+                jnp.concatenate(rows_chunk(layer, z), axis=1), WP[layer, 256:384, z * 1024:(z + 1) * 1024], LANES,
+                preferred_element_type=F32,
+            )
+        put_projected(acc * factor, SB2.at[layer])
+        exchange_start(2 * layer + 1, SB2.at[layer], RB2.at[layer])
 
     def active_rows():
         row = lax.broadcasted_iota(jnp.int32, (32, 32), 0)
@@ -239,30 +263,33 @@
         spread = jnp.broadcast_to(lens[0:1, :], (32, 32))
         return jnp.sum(jnp.where(row == col, spread, 0), axis=1, keepdims=True) > STEP
 
-    def wide128(value):
-        return jnp.concatenate([value, jnp.zeros_like(value)], axis=1)
+    low = lax.broadcasted_iota(jnp.int32, (32, 128), 1) < 64
+
+    def swap(value):
+        return pltpu.roll(value, 64, 1)
 
     def recur(layer):
         active = active_rows()
-        values, gates, first_sums, second_sums = [], [], [], []
+        first_sums, second_sums = [], []
         for h in range(4):
-            take = lambda kind: RB[layer, h, :, kind * 64:(kind + 1) * 64].astype(F32)
-            recept, key, value, dpre, rpre, gpre = [take(kind) for kind in range(6)]
             cols = slice(h * 64, (h + 1) * 64)
-            decay = jnp.exp(-(0.6065306597126334 * jax.nn.sigmoid(dbase[layer:layer + 1, cols] + dpre)))
-            rate = jax.nn.sigmoid(rbase[layer:layer + 1, cols] + rpre)
-            norm = jnp.sqrt(jnp.sum(key * key, axis=1, keepdims=True))
-            unit = key / jnp.maximum(norm, 1e-12)
-            up, kp = unit * rate, key * rate
-            first_sums.append(jnp.broadcast_to(jnp.sum(up * recept, axis=1, keepdims=True), (32, 64)))
-            second_sums.append(jnp.broadcast_to(jnp.sum(kp * recept, axis=1, keepdims=True), (32, 64)))
-            values.append(value)
-            gates.append(jax.nn.sigmoid(gpre))
-            V8[pl.ds(h, 32, stride=8), :] = wide128(-unit)
-            V8[pl.ds(4 + h, 32, stride=8), :] = wide128(decay * recept)
-            PQ[pl.ds(h, 32, stride=8), :] = wide128(jnp.where(active, up, 0.0))
-            PQ[pl.ds(4 + h, 32, stride=8), :] = wide128(jnp.where(active, kp, 0.0))
-            DEC[pl.ds(h, 32, stride=8), :] = wide128(jnp.where(active, decay, 1.0))
+            base = jnp.concatenate([dbase[layer:layer + 1, cols], rbase[layer:layer + 1, cols]], axis=1)
+            rec_key = RA4[layer, h, :, 0:128].astype(F32)
+            opened = jax.nn.sigmoid(base + RA4[layer, h, :, 128:256].astype(F32))
+            dec_rate = jnp.where(low, jnp.exp(-0.6065306597126334 * opened), opened)
+            both = rec_key * dec_rate
+            key_rec = swap(rec_key)
+            square = jnp.sum(jnp.where(low, key_rec * key_rec, 0.0), axis=1, keepdims=True)
+            scale = 1.0 / jnp.maximum(jnp.sqrt(square), 1e-12)
+            total = jnp.sum(jnp.where(low, 0.0, both * key_rec), axis=1, keepdims=True)
+            first_sums.append(total * scale)
+            second_sums.append(total)
+            V8[pl.ds(h, 32, stride=8), :] = key_rec * -scale
+            V8[pl.ds(4 + h, 32, stride=8), :] = both
+            key_rate = jnp.where(active, swap(both), 0.0)
+            PQ[pl.ds(h, 32, stride=8), :] = key_rate * scale
+            PQ[pl.ds(4 + h, 32, stride=8), :] = key_rate
+            DEC[pl.ds(h, 32, stride=8), :] = jnp.where(active, dec_rate, 1.0)
         for b in range(32):
             got = lax.dot_general(
                 V8[b * 8:(b + 1) * 8, 0:64].astype(BF16),
@@ -271,31 +298,33 @@
             )
             for half in range(2):
                 M2[half, b * 8:(b + 1) * 8, :] = got[:, half * 128:(half + 1) * 128]
-        low = lax.broadcasted_iota(jnp.int32, (32, 128), 1) < 64
+        exchange_done(2 * layer + 1, RB2.at[layer])
 
         def heads(base):
-            return jnp.concatenate([
-                jnp.where(low, M2[half, pl.ds(base + 2 * half, 32, stride=8), :],
-                          M2[half, pl.ds(base + 2 * half + 1, 32, stride=8), :])
-                for half in range(2)
-            ], axis=1)
-
-        sa, direct = heads(0), heads(4)
-        value = jnp.concatenate(values, axis=1)
-        SA[...] = sa
-        VA[...] = value
-        readout = direct + sa * jnp.concatenate(first_sums, axis=1) + value * jnp.concatenate(second_sums, axis=1)
-        normal = []
-        for h in range(4):
-            seg = readout[:, h * 64:(h + 1) * 64]
-            seg = seg - jnp.sum(seg, axis=1, keepdims=True) * (1.0 / 64)
-            spread = jnp.sum(seg * seg, axis=1, keepdims=True) * (1.0 / 64)
-            normal.append(seg * lax.rsqrt(spread + GROUP_EPS))
-        rows = jnp.concatenate(normal, axis=1) * ggain[layer:layer + 1, :] * jnp.concatenate(gates, axis=1)
-        rows = jnp.where(active, rows, 0.0).astype(BF16)
-        for q in range(4):
-            rh, ch = q // 2, q % 2
-            GP[layer, tp, q] = rows[rh * 16:(rh + 1) * 16, ch * 128:(ch + 1) * 128]
+            return jnp.where(low, M2[base // 2 % 2, pl.ds(base, 32, stride=8), :],
+                             M2[base // 2 % 2, pl.ds(base + 1, 32, stride=8), :])
+
+        for half in range(2):
+            even, odd = 2 * half, 2 * half + 1
+            even_vg, odd_vg = RB2[layer, even].astype(F32), RB2[layer, odd].astype(F32)
+            value = jnp.where(low, even_vg, swap(odd_vg))
+            gate = jax.nn.sigmoid(jnp.where(low, swap(even_vg), odd_vg))
+            sa, direct = heads(even), heads(4 + even)
+            half_cols = slice(half * 128, (half + 1) * 128)
+            SA[:, half_cols] = sa
+            VA[:, half_cols] = value
+            readout = (direct + sa * jnp.where(low, first_sums[even], first_sums[odd])
+                       + value * jnp.where(low, second_sums[even], second_sums[odd]))
+
+            def head_mean(data):
+                return jnp.where(low, jnp.sum(jnp.where(low, data, 0.0), axis=1, keepdims=True),
+                                 jnp.sum(jnp.where(low, 0.0, data), axis=1, keepdims=True)) * (1.0 / 64)
+
+            readout = readout - head_mean(readout)
+            normal = readout * lax.rsqrt(head_mean(readout * readout) + GROUP_EPS)
+            rows = jnp.where(active, normal * ggain[layer:layer + 1, half_cols] * gate, 0.0).astype(BF16)
+            for rh in range(2):
+                GP[layer][tp, rh * 2 + half] = rows[rh * 16:(rh + 1) * 16, :]
 
     head_of = lax.broadcasted_iota(jnp.int32, (8, 256), 1) // 64
     row_of = lax.broadcasted_iota(jnp.int32, (8, 256), 0)
@@ -314,27 +343,14 @@
                                    + delta[h * 64:(h + 1) * 64, :])
 
     def plane_first(layer):
-        here = GP.at[layer, tp]
+        here = GP[layer].at[tp]
         for hop_z in (2, 1, 3, 0):
             for hop_y in (2, 1, 3, 0):
                 if hop_z or hop_y:
                     send(here, p_send.at[layer], p_recv.at[layer], z=hop_z, y=hop_y)
 
     def plane_last(layer):
-        landed(GP.at[layer, pl.ds(0, 15)], p_recv.at[layer])
-
-    def output(layer):
-        acc = jnp.zeros((32, 256), F32)
-        for z in range(4):
-            parts = [
-                jnp.concatenate([GP[layer, z * 4 + y, ch], GP[layer, z * 4 + y, 2 + ch]], axis=0)
-                for y in range(4) for ch in range(2)
-            ]
-            acc += lax.dot_general(
-                jnp.concatenate(parts, axis=1), WO[layer, :, z * 1024:(z + 1) * 1024], LANES,
-                preferred_element_type=F32,
-            )
-        return acc.astype(BF16)
+        landed(GP[layer].at[pl.ds(0, 15)], p_recv.at[layer])
 
     gather_first(0)
     projections_out(0)
@@ -348,11 +364,10 @@
     projections_in(0)
     gather_last(0)
     project(0)
-    exchange_start(0, SB.at[0], RB.at[0])
     output_to_partner(0)
     projections_out(1)
     output_to_partner(1)
-    exchange_done(0, RB.at[0])
+    exchange_done(0, RA4.at[0])
     output_pass_on(0)
     landed(ST.at[0], st_sem.at[0])
     recur(0)
@@ -361,7 +376,7 @@
     projections_in(1)
     output_in(0)
     plane_last(0)
-    out = output(0)
+    out = output_product(GP0, WO0)
     for q in range(4):
         rh, ch = q // 2, q % 2
         G[1, q, at["z"], at["y"], at["x"]] = out[rh * 16:(rh + 1) * 16, ch * 128:(ch + 1) * 128]
@@ -370,8 +385,7 @@
     gather_middle(1)
     gather_last(1)
     project(1)
-    exchange_start(1, SB.at[1], RB.at[1])
-    exchange_done(1, RB.at[1])
+    exchange_done(2, RA4.at[1])
     output_pass_on(1)
     landed(ST.at[1], st_sem.at[1])
     recur(1)
@@ -379,43 +393,44 @@
     update(1, 0, 32)
     output_in(1)
     plane_last(1)
-    mixed[...] = output(1)
     for a in range(2):
         gather_sent(a)
-        exchange_sent(a, SB.at[a])
-        landed(GP.at[a, pl.ds(0, 15)], p_send.at[a])
+        exchange_sent(2 * a, SA4.at[a])
+        exchange_sent(2 * a + 1, SB2.at[a])
+        landed(GP[a].at[pl.ds(0, 15)], p_send.at[a])
     weights_sent()
 
 
-def finish_kernel(state_in, mixed_in, state_out, mixed_out, sem):
-    copies = [
-        pltpu.make_async_copy(state_in.at[0], state_out.at[0], sem.at[0]),
-        pltpu.make_async_copy(state_in.at[1], state_out.at[1], sem.at[1]),
-        pltpu.make_async_copy(mixed_in, mixed_out, sem.at[2]),
-    ]
+def finish_kernel(state_in, rows, weight, state_out, mixed_out, mixed, sem):
+    copies = [pltpu.make_async_copy(state_in.at[layer], state_out.at[layer], sem.at[layer]) for layer in range(2)]
     for copy in copies:
         copy.start()
+    mixed[...] = output_product(rows, weight)
+    copies.append(pltpu.make_async_copy(mixed, mixed_out, sem.at[2]))
+    copies[2].start()
     for copy in copies:
         copy.wait()
 
 
 def local(tokens, lengths, norm_gain, w_recept, w_key, w_value, w_decay, w_rate, w_gate, w_out,
           decay_base, rate_base, group_gain, state):
-    weights = [jnp.swapaxes(w, 1, 2) for w in (w_recept, w_key, w_value, w_decay, w_rate, w_gate, w_out)]
+    weights = [jnp.swapaxes(w, 1, 2) for w in (w_recept, w_key, w_decay, w_rate, w_value, w_gate, w_out)]
     hbm = pl.BlockSpec(memory_space=pltpu.HBM)
     vmem = pl.BlockSpec(memory_space=pltpu.VMEM)
-    mixed, stepped = pl.pallas_call(
+    stepped, rows, columns = pl.pallas_call(
         step_kernel,
-        out_shape=(pltpu.VMEM((32, 256), BF16), pltpu.VMEM(state.shape, F32)),
+        out_shape=(pltpu.VMEM(state.shape, F32), pltpu.VMEM((16, 4, 16, 128), BF16), pltpu.VMEM((256, 4096), BF16)),
         in_specs=[hbm] * 14,
-        out_specs=(vmem, vmem),
+        out_specs=(vmem, vmem, vmem),
         scratch_shapes=[
             pltpu.VMEM((2, 4, 4, 4, 4, 16, 128), BF16),
-            pltpu.VMEM((2, 16, 4, 16, 128), BF16),
+            pltpu.VMEM((16, 4, 16, 128), BF16),
             pltpu.VMEM((2, 384, 4096), BF16),
-            pltpu.VMEM((2, 256, 4096), BF16),
-            pltpu.VMEM((2, 4, 32, 384), BF16),
-            pltpu.VMEM((2, 4, 32, 384), BF16),
+            pltpu.VMEM((256, 4096), BF16),
+            pltpu.VMEM((2, 4, 32, 256), BF16),
+            pltpu.VMEM((2, 4, 32, 256), BF16),
+            pltpu.VMEM((2, 4, 32, 128), BF16),
+            pltpu.VMEM((2, 4, 32, 128), BF16),
             pltpu.VMEM((256, 128), F32),
             pltpu.VMEM((2, 256, 128), F32),
             pltpu.VMEM((32, 256), F32),
@@ -431,8 +446,8 @@
             pltpu.SemaphoreType.DMA((2, 4, 5)),
             pltpu.SemaphoreType.DMA((2,)),
             pltpu.SemaphoreType.DMA((2,)),
-            pltpu.SemaphoreType.DMA((2,)),
-            pltpu.SemaphoreType.DMA((2,)),
+            pltpu.SemaphoreType.DMA((4,)),
+            pltpu.SemaphoreType.DMA((4,)),
             pltpu.SemaphoreType.DMA((2,)),
             pltpu.SemaphoreType.DMA((2,)),
             pltpu.SemaphoreType.DMA((2,)),
@@ -441,18 +456,18 @@
             pltpu.SemaphoreType.DMA((4,)),
             pltpu.SemaphoreType.DMA((5,)),
         ],
-        compiler_params=pltpu.CompilerParams(collective_id=0, has_side_effects=True, vmem_limit_bytes=52 << 20),
+        compiler_params=pltpu.CompilerParams(collective_id=0, has_side_effects=True, vmem_limit_bytes=44 << 20),
         name="decode_step",
     )(tokens, lengths.reshape(1, 32), norm_gain, *weights, decay_base, rate_base, group_gain, state)
     new_state, mixed = pl.pallas_call(
         finish_kernel,
         out_shape=(pltpu.HBM(state.shape, F32), pltpu.HBM((32, 256), BF16)),
-        in_specs=[vmem, vmem],
+        in_specs=[vmem] * 3,
         out_specs=(hbm, hbm),
-        scratch_shapes=[pltpu.SemaphoreType.DMA((3,))],
-        compiler_params=pltpu.CompilerParams(vmem_limit_bytes=1 << 20),
+        scratch_shapes=[pltpu.VMEM((32, 256), BF16), pltpu.SemaphoreType.DMA((3,))],
+        compiler_params=pltpu.CompilerParams(vmem_limit_bytes=4 << 20),
         name="finish",
-    )(stepped, mixed)
+    )(stepped, rows, columns)
     return mixed, new_state
 
 

time: 63.2 us -> 60.8 us (0.962)
  Pallas kernels: 62.4 us -> 60 us
    pallas_call x1, Pallas kernels: 59 us -> 56.6 us  [local(): pl.pallas_call(step_kernel, out_shape=(pltpu.VMEM(state.shape, F32), pltp...]
where the time goes in v5:
time: 60.8 us; the launch traced here: 60.6 us
  Pallas kernels  60 us (99%)
  between operations  0.64 us (1%)
    pallas_call x1, Pallas kernels, local(): pl.pallas_call(step_kernel, out_shape=(pltpu.VMEM(state.shape, F32), pltp...  56.6 us
    pallas_call x1, Pallas kernels, local(): pl.pallas_call(finish_kernel, out_shape=(pltpu.HBM(state.shape, F32), plt...  3.42 us

profile of v5, /device:TPU:0, one launch (start us, length us, event | category | flops | bytes accessed | tf_op | source)
XLA Modules:
  0.0 60.6 jit_solution(17688745140842945165)
XLA Ops:
  0.6 56.6 %decode_step.1 = (f32[2,32,4,64,64]{4,3,2,1,0:T(8,128)S(1)}, bf16[16,4,16,128]{3,2,1,0:T(8,128)(2,1)S(1)}, bf16[256,4096]{1,0:T(8,128)(2,1)S(1)}) custom-call(bf16[32,256]{1,0:T(8,128)(2,1)} %tok.1, s32[1,32]{1,0:T(1,128)} %bitcast.15, f32[2,4096]{1,0:T(2,128)} %gain_in.1, bf16[2,32,4096]{2,1,0:T(8,128)(2,1)} %bitcast.8, bf16[2,32,4096]{2,1,0:T(8,128)(2,1)} %bitcast.9, ...), custom_call_target="tpu_custom_call" | custom-call | tf_op jit(solution)/shard_map/decode_step/pallas_call | solution.py:420
  57.2 3.4 %finish.1 = (f32[2,32,4,64,64]{4,3,2,1,0:T(8,128)}, bf16[32,256]{1,0:T(8,128)(2,1)}) custom-call(f32[2,32,4,64,64]{4,3,2,1,0:T(8,128)S(1)} %get-tuple-element.7.state_in, bf16[16,4,16,128]{3,2,1,0:T(8,128)(2,1)S(1)} %get-tuple-element.8.rows, bf16[256,4096]{1,0:T(8,128)(2,1)S(1)} %get-tuple-element.9.weight), custom_call_target="tpu_custom_call" | custom-call | tf_op jit(solution)/shard_map/finish/pallas_call | solution.py:462

commit v6 on v5

--- a/solution.py
+++ b/solution.py
@@ -18,15 +18,16 @@
 ROWS = (((0,), (0,)), ((), ()))
 
 
-def output_product(rows, weight):
+def output_product(rows, weight, planes):
     acc = jnp.zeros((32, 256), F32)
-    for z in range(4):
+    for plane in planes:
+        z = plane()
         parts = [
             jnp.concatenate([rows[z * 4 + y, ch], rows[z * 4 + y, 2 + ch]], axis=0)
             for y in range(4) for ch in range(2)
         ]
         acc += lax.dot_general(
-            jnp.concatenate(parts, axis=1), weight[:, z * 1024:(z + 1) * 1024], LANES,
+            jnp.concatenate(parts, axis=1), weight[:, pl.ds(pl.multiple_of(z * 1024, 1024), 1024)], LANES,
             preferred_element_type=F32,
         )
     return acc.astype(BF16)
@@ -121,18 +122,18 @@
             first, second, third = ORDERS[q]
             landed(G.at[a, q, 0, 0, pl.ds(0, 3)], g_recv.at[a, q, 0])
             for on in (2, 1, 3):
-                send(block(a, q, first), g_send.at[a, q, 2], g_recv.at[a, q, 4], **{third: on})
+                send(block(a, q, first), g_send.at[a, q, 2], g_recv.at[a, q, 3 + on], **{third: on})
         for over in (1, 3, 2):
             for q in range(4):
                 first, second, third = ORDERS[q]
                 landed(G.at[a, q, 0, 0], g_recv.at[a, q, over])
                 line = {second: (at[second] + 4 - over) % 4}
                 for on in (2, 1, 3):
-                    send(block(a, q, first, line), g_send.at[a, q, 2], g_recv.at[a, q, 4], **{third: on})
-
-    def gather_last(a):
+                    send(block(a, q, first, line), g_send.at[a, q, 2], g_recv.at[a, q, 3 + on], **{third: on})
+
+    def gather_last(a, on):
         for q in range(4):
-            landed(G.at[a, q, pl.ds(0, 3)], g_recv.at[a, q, 4])
+            landed(G.at[a, q, 0], g_recv.at[a, q, 3 + on])
 
     def gather_sent(a):
         for q in range(4):
@@ -236,15 +237,26 @@
     def project(layer):
         squares = jnp.zeros((128, 128), F32)
         acc = jnp.zeros((128, 256), F32)
-        for z in range(4):
-            parts = rows_chunk(layer, z)
-            for part in parts:
-                wide = part.astype(F32)
-                squares += wide * wide
-            acc += lax.dot_general(
-                jnp.concatenate(parts, axis=1), WP[layer, 0:256, z * 1024:(z + 1) * 1024], LANES,
-                preferred_element_type=F32,
-            )
+        for on in (0, 1, 3, 2):
+            if on:
+                gather_last(layer, on)
+            for ch in range(2):
+                along = ORDERS[ch][2]
+                came = (at[along] + 4 - on) % 4
+                spots = [(came, other) if along == "z" else (other, came) for other in range(4)]
+                parts, weights = [], []
+                for z, y in spots:
+                    parts.append(jnp.concatenate(
+                        [G[layer, rh * 2 + ch, z, y].reshape(64, 128) for rh in range(2)], axis=0))
+                    start = pl.multiple_of(z * 1024 + y * 256 + ch * 128, 128)
+                    weights.append(WP[layer, 0:256, pl.ds(start, 128)])
+                for part in parts:
+                    wide = part.astype(F32)
+                    squares += wide * wide
+                acc += lax.dot_general(
+                    jnp.concatenate(parts, axis=1), jnp.concatenate(weights, axis=1), LANES,
+                    preferred_element_type=F32,
+                )
         factor = lax.rsqrt(jnp.sum(squares, axis=1, keepdims=True) * (1.0 / 4096) + RMS_EPS)
         put_projected(acc * factor, SA4.at[layer])
         exchange_start(2 * layer, SA4.at[layer], RA4.at[layer])
@@ -347,10 +359,10 @@
         for hop_z in (2, 1, 3, 0):
             for hop_y in (2, 1, 3, 0):
                 if hop_z or hop_y:
-                    send(here, p_send.at[layer], p_recv.at[layer], z=hop_z, y=hop_y)
-
-    def plane_last(layer):
-        landed(GP[layer].at[pl.ds(0, 15)], p_recv.at[layer])
+                    send(here, p_send.at[layer], p_recv.at[layer, hop_z], z=hop_z, y=hop_y)
+
+    def plane_last(layer, hop_z):
+        landed(GP[layer].at[pl.ds(0, 4 if hop_z else 3)], p_recv.at[layer, hop_z])
 
     gather_first(0)
     projections_out(0)
@@ -362,7 +374,6 @@
     for copy in small:
         copy.wait()
     projections_in(0)
-    gather_last(0)
     project(0)
     output_to_partner(0)
     projections_out(1)
@@ -375,15 +386,18 @@
     update(0, 0, 32)
     projections_in(1)
     output_in(0)
-    plane_last(0)
-    out = output_product(GP0, WO0)
+
+    def came(hop_z):
+        plane_last(0, hop_z)
+        return (at["z"] + 4 - hop_z) % 4
+
+    out = output_product(GP0, WO0, [functools.partial(came, hop_z) for hop_z in (0, 1, 3, 2)])
     for q in range(4):
         rh, ch = q // 2, q % 2
         G[1, q, at["z"], at["y"], at["x"]] = out[rh * 16:(rh + 1) * 16, ch * 128:(ch + 1) * 128]
     gather_first(1)
     output_over_x(1)
     gather_middle(1)
-    gather_last(1)
     project(1)
     exchange_done(2, RA4.at[1])
     output_pass_on(1)
@@ -392,7 +406,8 @@
     plane_first(1)
     update(1, 0, 32)
     output_in(1)
-    plane_last(1)
+    for hop_z in range(4):
+        plane_last(1, hop_z)
     for a in range(2):
         gather_sent(a)
         exchange_sent(2 * a, SA4.at[a])
@@ -405,7 +420,7 @@
     copies = [pltpu.make_async_copy(state_in.at[layer], state_out.at[layer], sem.at[layer]) for layer in range(2)]
     for copy in copies:
         copy.start()
-    mixed[...] = output_product(rows, weight)
+    mixed[...] = output_product(rows, weight, [functools.partial(int, z) for z in range(4)])
     copies.append(pltpu.make_async_copy(mixed, mixed_out, sem.at[2]))
     copies[2].start()
     for copy in copies:
@@ -443,9 +458,9 @@
             pltpu.VMEM((2, 256), F32),
             pltpu.VMEM((2, 256), F32),
             pltpu.SemaphoreType.DMA((2, 4, 3)),
-            pltpu.SemaphoreType.DMA((2, 4, 5)),
+            pltpu.SemaphoreType.DMA((2, 4, 7)),
             pltpu.SemaphoreType.DMA((2,)),
-            pltpu.SemaphoreType.DMA((2,)),
+            pltpu.SemaphoreType.DMA((2, 4)),
             pltpu.SemaphoreType.DMA((4,)),
             pltpu.SemaphoreType.DMA((4,)),
             pltpu.SemaphoreType.DMA((2,)),

time: 60.8 us -> 60.1 us (0.988)
  Pallas kernels: 60 us -> 59.3 us
    pallas_call x1, Pallas kernels: 56.6 us -> 55.9 us  [local(): pl.pallas_call(step_kernel, out_shape=(pltpu.VMEM(state.shape, F32), pltp...]
where the time goes in v6:
time: 60.1 us; the launch traced here: 60 us
  Pallas kernels  59.3 us (99%)
  between operations  0.64 us (1%)
    pallas_call x1, Pallas kernels, local(): pl.pallas_call(step_kernel, out_shape=(pltpu.VMEM(state.shape, F32), pltp...  55.9 us
    pallas_call x1, Pallas kernels, local(): pl.pallas_call(finish_kernel, out_shape=(pltpu.HBM(state.shape, F32), plt...  3.42 us

profile of v6, /device:TPU:0, one launch (start us, length us, event | category | flops | bytes accessed | tf_op | source)
XLA Modules:
  0.0 60.0 jit_solution(13379660675411918231)
XLA Ops:
  0.6 55.9 %decode_step.1 = (f32[2,32,4,64,64]{4,3,2,1,0:T(8,128)S(1)}, bf16[16,4,16,128]{3,2,1,0:T(8,128)(2,1)S(1)}, bf16[256,4096]{1,0:T(8,128)(2,1)S(1)}) custom-call(bf16[32,256]{1,0:T(8,128)(2,1)} %tok.1, s32[1,32]{1,0:T(1,128)} %bitcast.15, f32[2,4096]{1,0:T(2,128)} %gain_in.1, bf16[2,32,4096]{2,1,0:T(8,128)(2,1)} %bitcast.8, bf16[2,32,4096]{2,1,0:T(8,128)(2,1)} %bitcast.9, ...), custom_call_target="tpu_custom_call" | custom-call | tf_op jit(solution)/shard_map/decode_step/pallas_call | solution.py:435
  56.5 3.4 %finish.1 = (f32[2,32,4,64,64]{4,3,2,1,0:T(8,128)}, bf16[32,256]{1,0:T(8,128)(2,1)}) custom-call(f32[2,32,4,64,64]{4,3,2,1,0:T(8,128)S(1)} %get-tuple-element.7.state_in, bf16[16,4,16,128]{3,2,1,0:T(8,128)(2,1)S(1)} %get-tuple-element.8.rows, bf16[256,4096]{1,0:T(8,128)(2,1)S(1)} %get-tuple-element.9.weight), custom_call_target="tpu_custom_call" | custom-call | tf_op jit(solution)/shard_map/finish/pallas_call | solution.py:477

commit v7 on v6

--- a/solution.py
+++ b/solution.py
@@ -123,6 +123,8 @@
             landed(G.at[a, q, 0, 0, pl.ds(0, 3)], g_recv.at[a, q, 0])
             for on in (2, 1, 3):
                 send(block(a, q, first), g_send.at[a, q, 2], g_recv.at[a, q, 3 + on], **{third: on})
+        if a == 0:
+            output_over_x(0)
         for over in (1, 3, 2):
             for q in range(4):
                 first, second, third = ORDERS[q]
@@ -176,23 +178,33 @@
 
     def output_over_x(layer):
         for part in range(4):
-            for hop in (2, 1, 3):
+            for hop in (1, 3):
                 pltpu.make_async_remote_copy(
                     src_ref=w_out.at[layer, pl.ds(part * 8, 8)],
                     dst_ref=WO[layer].at[pl.ds(pl.multiple_of(own_cols + part * 8, 8), 8)],
-                    send_sem=o_sem.at[layer, 1], recv_sem=o_sem.at[layer, 2],
+                    send_sem=o_sem.at[layer, 1], recv_sem=o_sem.at[layer, 1 + hop],
                     device_id=device(x=hop), device_id_type=MESH,
                 ).start()
+
+    def output_far_x(layer):
+        for half, hop in enumerate((1, 3)):
+            landed(WO[layer].at[pl.ds(0, 32)], o_sem.at[layer, 1 + hop])
+            cols = pl.ds(pl.multiple_of((at["x"] + 4 - hop) % 4 * 64 + c * 32 + half * 16, 16), 16)
+            pltpu.make_async_remote_copy(
+                src_ref=WO[layer].at[cols], dst_ref=WO[layer].at[cols],
+                send_sem=o_sem.at[layer, 7], recv_sem=o_sem.at[layer, 8],
+                device_id=device(x=hop), device_id_type=MESH,
+            ).start()
 
     def output_to_partner(layer):
         pltpu.make_async_remote_copy(
             src_ref=w_out.at[layer], dst_ref=WO[layer].at[pl.ds(own_cols, 32)],
-            send_sem=o_sem.at[layer, 3], recv_sem=o_sem.at[layer, 4],
+            send_sem=o_sem.at[layer, 3], recv_sem=o_sem.at[layer, 9],
             device_id=partner, device_id_type=MESH,
         ).start()
 
     def output_pass_on(layer):
-        landed(WO[layer].at[pl.ds(0, 96)], o_sem.at[layer, 2])
+        landed(WO[layer].at[pl.ds(0, 32)], o_sem.at[layer, 8])
         for hop in (1, 2, 3):
             cols = pl.ds(pl.multiple_of(((at["x"] + hop) % 4) * 64 + c * 32, 32), 32)
             pltpu.make_async_remote_copy(
@@ -203,11 +215,12 @@
 
     def output_in(layer):
         landed(WO[layer].at[pl.ds(0, 32)], o_sem.at[layer, 0])
-        landed(WO[layer].at[pl.ds(0, 32)], o_sem.at[layer, 4])
+        landed(WO[layer].at[pl.ds(0, 32)], o_sem.at[layer, 9])
         landed(WO[layer].at[pl.ds(0, 96)], o_sem.at[layer, 6])
 
     def output_sent(layer):
-        landed(WO[layer].at[pl.ds(0, 96)], o_sem.at[layer, 1])
+        landed(WO[layer].at[pl.ds(0, 64)], o_sem.at[layer, 1])
+        landed(WO[layer].at[pl.ds(0, 32)], o_sem.at[layer, 7])
         landed(WO[layer].at[pl.ds(0, 32)], o_sem.at[layer, 3])
         landed(WO[layer].at[pl.ds(0, 96)], o_sem.at[layer, 5])
 
@@ -367,7 +380,6 @@
     gather_first(0)
     projections_out(0)
     pltpu.make_async_copy(state.at[0], ST.at[0], st_sem.at[0]).start()
-    output_over_x(0)
     weights_local(1)
     pltpu.make_async_copy(state.at[1], ST.at[1], st_sem.at[1]).start()
     gather_middle(0)
@@ -375,14 +387,15 @@
         copy.wait()
     projections_in(0)
     project(0)
+    output_far_x(0)
     output_to_partner(0)
     projections_out(1)
     output_to_partner(1)
     exchange_done(0, RA4.at[0])
-    output_pass_on(0)
     landed(ST.at[0], st_sem.at[0])
     recur(0)
     plane_first(0)
+    output_pass_on(0)
     update(0, 0, 32)
     projections_in(1)
     output_in(0)
@@ -396,14 +409,15 @@
         rh, ch = q // 2, q % 2
         G[1, q, at["z"], at["y"], at["x"]] = out[rh * 16:(rh + 1) * 16, ch * 128:(ch + 1) * 128]
     gather_first(1)
+    gather_middle(1)
     output_over_x(1)
-    gather_middle(1)
     project(1)
+    output_far_x(1)
     exchange_done(2, RA4.at[1])
-    output_pass_on(1)
     landed(ST.at[1], st_sem.at[1])
     recur(1)
     plane_first(1)
+    output_pass_on(1)
     update(1, 0, 32)
     output_in(1)
     for hop_z in range(4):
@@ -466,7 +480,7 @@
             pltpu.SemaphoreType.DMA((2,)),
             pltpu.SemaphoreType.DMA((2,)),
             pltpu.SemaphoreType.DMA((2,)),
-            pltpu.SemaphoreType.DMA((2, 7)),
+            pltpu.SemaphoreType.DMA((2, 10)),
             pltpu.SemaphoreType.DMA((2,)),
             pltpu.SemaphoreType.DMA((4,)),
             pltpu.SemaphoreType.DMA((5,)),

time: 60.1 us -> 57.6 us (0.958)
  Pallas kernels: 59.3 us -> 56.9 us
    pallas_call x1, Pallas kernels: 55.9 us -> 53.5 us  [local(): pl.pallas_call(step_kernel, out_shape=(pltpu.VMEM(state.shape, F32), pltp...]
where the time goes in v7:
time: 57.6 us; the launch traced here: 57.5 us
  Pallas kernels  56.9 us (99%)
  between operations  0.64 us (1%)
    pallas_call x1, Pallas kernels, local(): pl.pallas_call(step_kernel, out_shape=(pltpu.VMEM(state.shape, F32), pltp...  53.5 us
    pallas_call x1, Pallas kernels, local(): pl.pallas_call(finish_kernel, out_shape=(pltpu.HBM(state.shape, F32), plt...  3.42 us

profile of v7, /device:TPU:0, one launch (start us, length us, event | category | flops | bytes accessed | tf_op | source)
XLA Modules:
  0.0 57.5 jit_solution(860691497030661826)
XLA Ops:
  0.6 53.5 %decode_step.1 = (f32[2,32,4,64,64]{4,3,2,1,0:T(8,128)S(1)}, bf16[16,4,16,128]{3,2,1,0:T(8,128)(2,1)S(1)}, bf16[256,4096]{1,0:T(8,128)(2,1)S(1)}) custom-call(bf16[32,256]{1,0:T(8,128)(2,1)} %tok.1, s32[1,32]{1,0:T(1,128)} %bitcast.15, f32[2,4096]{1,0:T(2,128)} %gain_in.1, bf16[2,32,4096]{2,1,0:T(8,128)(2,1)} %bitcast.8, bf16[2,32,4096]{2,1,0:T(8,128)(2,1)} %bitcast.9, ...), custom_call_target="tpu_custom_call" | custom-call | tf_op jit(solution)/shard_map/decode_step/pallas_call | solution.py:449
  54.1 3.4 %finish.1 = (f32[2,32,4,64,64]{4,3,2,1,0:T(8,128)}, bf16[32,256]{1,0:T(8,128)(2,1)}) custom-call(f32[2,32,4,64,64]{4,3,2,1,0:T(8,128)S(1)} %get-tuple-element.7.state_in, bf16[16,4,16,128]{3,2,1,0:T(8,128)(2,1)S(1)} %get-tuple-element.8.rows, bf16[256,4096]{1,0:T(8,128)(2,1)S(1)} %get-tuple-element.9.weight), custom_call_target="tpu_custom_call" | custom-call | tf_op jit(solution)/shard_map/finish/pallas_call | solution.py:491

commit v8 on v7

--- a/solution.py
+++ b/solution.py
@@ -13,7 +13,7 @@
 MESH = pl.DeviceIdType.MESH
 F32 = jnp.float32
 BF16 = jnp.bfloat16
-ORDERS = (("x", "y", "z"), ("x", "z", "y"), ("x", "y", "z"), ("x", "z", "y"))
+ORDERS = (("y", "x", "z"), ("z", "x", "y"), ("y", "x", "z"), ("z", "x", "y"))
 LANES = (((1,), (1,)), ((), ()))
 ROWS = (((0,), (0,)), ((), ()))
 
@@ -36,7 +36,7 @@
 def step_kernel(
     tok, lens_in, gain_in, w0, w1, w2, w3, w4, w5, w_out, dbase_in, rbase_in, ggain_in, state,
     ST, GP1, WO1,
-    G, GP0, WP, WO0, SA4, RA4, SB2, RB2, V8, M2, SA, VA, PQ, DEC, lens, gain, dbase, rbase, ggain,
+    G, GP0, WP, WO0, SA4, RA4, SB2, RB2, V8, M2, S16, SA, VA, PQ, DEC, lens, gain, dbase, rbase, ggain,
     g_send, g_recv, p_send, p_recv, a_send, a_recv, w_local, w_send, w_recv, o_sem, st_sem, tok_sem, small_sem,
 ):
     tp, dp = lax.axis_index("tp"), lax.axis_index("dp")
@@ -56,6 +56,7 @@
         dict(x=hx, y=hy, z=hz) for hx in range(4) for hy in range(4) for hz in range(4)
         if 0 in (hx, hy, hz) and (hx, hy, hz) != (0, 0, 0)
     ]
+    peers.sort(key=lambda peer: -sum(min(hop, 4 - hop) for hop in peer.values()))
     for peer in peers:
         pl.semaphore_signal(barrier, inc=1, device_id=device(**peer), device_id_type=MESH)
     pl.semaphore_signal(barrier, inc=1, device_id=partner, device_id_type=MESH)
@@ -293,6 +294,23 @@
     def swap(value):
         return pltpu.roll(value, 64, 1)
 
+    own_lanes = (lax.broadcasted_iota(jnp.int32, (32, 256), 0) // 8
+                 == lax.broadcasted_iota(jnp.int32, (32, 256), 1) // 64)
+
+    def pack(layer):
+        landed(ST.at[layer], st_sem.at[layer])
+
+        def four(group, carry):
+            for half in range(2):
+                even, odd = [
+                    ST[layer, group * 4 + half * 2 + i].reshape(256, 64) for i in range(2)
+                ]
+                both = jnp.concatenate([even, odd], axis=1)
+                S16[layer, group, :, half * 128:(half + 1) * 128] = both.astype(BF16)
+            return carry
+
+        lax.fori_loop(0, 8, four, 0)
+
     def recur(layer):
         active = active_rows()
         first_sums, second_sums = [], []
@@ -315,14 +333,13 @@
             PQ[pl.ds(h, 32, stride=8), :] = key_rate * scale
             PQ[pl.ds(4 + h, 32, stride=8), :] = key_rate
             DEC[pl.ds(h, 32, stride=8), :] = jnp.where(active, dec_rate, 1.0)
-        for b in range(32):
-            got = lax.dot_general(
-                V8[b * 8:(b + 1) * 8, 0:64].astype(BF16),
-                ST[layer, b].reshape(256, 64).astype(BF16), LANES,
-                preferred_element_type=F32,
-            )
+        for group in range(8):
+            vectors = V8[group * 32:(group + 1) * 32, :]
+            vectors = jnp.where(low, vectors, swap(vectors))
+            vectors = jnp.where(own_lanes, jnp.concatenate([vectors, vectors], axis=1), 0.0).astype(BF16)
+            got = lax.dot_general(vectors, S16[layer, group], LANES, preferred_element_type=F32)
             for half in range(2):
-                M2[half, b * 8:(b + 1) * 8, :] = got[:, half * 128:(half + 1) * 128]
+                M2[half, group * 32:(group + 1) * 32, :] = got[:, half * 128:(half + 1) * 128]
         exchange_done(2 * layer + 1, RB2.at[layer])
 
         def heads(base):
@@ -386,13 +403,13 @@
     for copy in small:
         copy.wait()
     projections_in(0)
+    pack(0)
     project(0)
     output_far_x(0)
     output_to_partner(0)
     projections_out(1)
     output_to_partner(1)
     exchange_done(0, RA4.at[0])
-    landed(ST.at[0], st_sem.at[0])
     recur(0)
     plane_first(0)
     output_pass_on(0)
@@ -411,10 +428,10 @@
     gather_first(1)
     gather_middle(1)
     output_over_x(1)
+    pack(1)
     project(1)
     output_far_x(1)
     exchange_done(2, RA4.at[1])
-    landed(ST.at[1], st_sem.at[1])
     recur(1)
     plane_first(1)
     output_pass_on(1)
@@ -462,6 +479,7 @@
             pltpu.VMEM((2, 4, 32, 128), BF16),
             pltpu.VMEM((256, 128), F32),
             pltpu.VMEM((2, 256, 128), F32),
+            pltpu.VMEM((2, 8, 256, 256), BF16),
             pltpu.VMEM((32, 256), F32),
             pltpu.VMEM((32, 256), F32),
             pltpu.VMEM((256, 128), F32),

time: 57.6 us -> 56.8 us (0.986)
  Pallas kernels: 56.9 us -> 56.1 us
    pallas_call x1, Pallas kernels: 53.5 us -> 52.7 us  [local(): pl.pallas_call(step_kernel, out_shape=(pltpu.VMEM(state.shape, F32), pltp...]
where the time goes in v8:
time: 56.8 us; the launch traced here: 56.7 us
  Pallas kernels  56.1 us (99%)
  between operations  0.64 us (1%)
    pallas_call x1, Pallas kernels, local(): pl.pallas_call(step_kernel, out_shape=(pltpu.VMEM(state.shape, F32), pltp...  52.7 us
    pallas_call x1, Pallas kernels, local(): pl.pallas_call(finish_kernel, out_shape=(pltpu.HBM(state.shape, F32), plt...  3.42 us

profile of v8, /device:TPU:0, one launch (start us, length us, event | category | flops | bytes accessed | tf_op | source)
XLA Modules:
  0.0 56.7 jit_solution(16993396172116564888)
XLA Ops:
  0.6 52.7 %decode_step.1 = (f32[2,32,4,64,64]{4,3,2,1,0:T(8,128)S(1)}, bf16[16,4,16,128]{3,2,1,0:T(8,128)(2,1)S(1)}, bf16[256,4096]{1,0:T(8,128)(2,1)S(1)}) custom-call(bf16[32,256]{1,0:T(8,128)(2,1)} %tok.1, s32[1,32]{1,0:T(1,128)} %bitcast.15, f32[2,4096]{1,0:T(2,128)} %gain_in.1, bf16[2,32,4096]{2,1,0:T(8,128)(2,1)} %bitcast.8, bf16[2,32,4096]{2,1,0:T(8,128)(2,1)} %bitcast.9, ...), custom_call_target="tpu_custom_call" | custom-call | tf_op jit(solution)/shard_map/decode_step/pallas_call | solution.py:466
  53.3 3.4 %finish.1 = (f32[2,32,4,64,64]{4,3,2,1,0:T(8,128)}, bf16[32,256]{1,0:T(8,128)(2,1)}) custom-call(f32[2,32,4,64,64]{4,3,2,1,0:T(8,128)S(1)} %get-tuple-element.7.state_in, bf16[16,4,16,128]{3,2,1,0:T(8,128)(2,1)S(1)} %get-tuple-element.8.rows, bf16[256,4096]{1,0:T(8,128)(2,1)S(1)} %get-tuple-element.9.weight), custom_call_target="tpu_custom_call" | custom-call | tf_op jit(solution)/shard_map/finish/pallas_call | solution.py:509

commit v9 on v8

--- a/solution.py
+++ b/solution.py
@@ -311,28 +311,37 @@
 
         lax.fori_loop(0, 8, four, 0)
 
+    def head_vectors(layer, h):
+        cols = slice(h * 64, (h + 1) * 64)
+        base = jnp.concatenate([dbase[layer:layer + 1, cols], rbase[layer:layer + 1, cols]], axis=1)
+        rec_key = RA4[layer, h, :, 0:128].astype(F32)
+        opened = jax.nn.sigmoid(base + RA4[layer, h, :, 128:256].astype(F32))
+        dec_rate = jnp.where(low, jnp.exp(-0.6065306597126334 * opened), opened)
+        both = rec_key * dec_rate
+        key_rec = swap(rec_key)
+        square = jnp.sum(jnp.where(low, key_rec * key_rec, 0.0), axis=1, keepdims=True)
+        scale = 1.0 / jnp.maximum(jnp.sqrt(square), 1e-12)
+        return dec_rate, both, key_rec, scale
+
+    def update_vectors(layer):
+        active = active_rows()
+        for h in range(4):
+            dec_rate, both, key_rec, scale = head_vectors(layer, h)
+            key_rate = jnp.where(active, swap(both), 0.0)
+            PQ[pl.ds(h, 32, stride=8), :] = key_rate * scale
+            PQ[pl.ds(4 + h, 32, stride=8), :] = key_rate
+            DEC[pl.ds(h, 32, stride=8), :] = jnp.where(active, dec_rate, 1.0)
+
     def recur(layer):
         active = active_rows()
         first_sums, second_sums = [], []
         for h in range(4):
-            cols = slice(h * 64, (h + 1) * 64)
-            base = jnp.concatenate([dbase[layer:layer + 1, cols], rbase[layer:layer + 1, cols]], axis=1)
-            rec_key = RA4[layer, h, :, 0:128].astype(F32)
-            opened = jax.nn.sigmoid(base + RA4[layer, h, :, 128:256].astype(F32))
-            dec_rate = jnp.where(low, jnp.exp(-0.6065306597126334 * opened), opened)
-            both = rec_key * dec_rate
-            key_rec = swap(rec_key)
-            square = jnp.sum(jnp.where(low, key_rec * key_rec, 0.0), axis=1, keepdims=True)
-            scale = 1.0 / jnp.maximum(jnp.sqrt(square), 1e-12)
+            dec_rate, both, key_rec, scale = head_vectors(layer, h)
             total = jnp.sum(jnp.where(low, 0.0, both * key_rec), axis=1, keepdims=True)
             first_sums.append(total * scale)
             second_sums.append(total)
             V8[pl.ds(h, 32, stride=8), :] = key_rec * -scale
             V8[pl.ds(4 + h, 32, stride=8), :] = both
-            key_rate = jnp.where(active, swap(both), 0.0)
-            PQ[pl.ds(h, 32, stride=8), :] = key_rate * scale
-            PQ[pl.ds(4 + h, 32, stride=8), :] = key_rate
-            DEC[pl.ds(h, 32, stride=8), :] = jnp.where(active, dec_rate, 1.0)
         for group in range(8):
             vectors = V8[group * 32:(group + 1) * 32, :]
             vectors = jnp.where(low, vectors, swap(vectors))
@@ -413,6 +422,7 @@
     recur(0)
     plane_first(0)
     output_pass_on(0)
+    update_vectors(0)
     update(0, 0, 32)
     projections_in(1)
     output_in(0)
@@ -435,6 +445,7 @@
     recur(1)
     plane_first(1)
     output_pass_on(1)
+    update_vectors(1)
     update(1, 0, 32)
     output_in(1)
     for hop_z in range(4):

time: 56.8 us -> 56.8 us (level)
  no operation moved by 1% of the time
where the time goes in v9:
time: 56.8 us; the launch traced here: 56.7 us
  Pallas kernels  56.1 us (99%)
  between operations  0.64 us (1%)
    pallas_call x1, Pallas kernels, local(): pl.pallas_call(step_kernel, out_shape=(pltpu.VMEM(state.shape, F32), pltp...  52.7 us
    pallas_call x1, Pallas kernels, local(): pl.pallas_call(finish_kernel, out_shape=(pltpu.HBM(state.shape, F32), plt...  3.42 us

profile of v9, /device:TPU:0, one launch (start us, length us, event | category | flops | bytes accessed | tf_op | source)
XLA Modules:
  0.0 56.7 jit_solution(10625773862076342837)
XLA Ops:
  0.6 52.7 %decode_step.1 = (f32[2,32,4,64,64]{4,3,2,1,0:T(8,128)S(1)}, bf16[16,4,16,128]{3,2,1,0:T(8,128)(2,1)S(1)}, bf16[256,4096]{1,0:T(8,128)(2,1)S(1)}) custom-call(bf16[32,256]{1,0:T(8,128)(2,1)} %tok.1, s32[1,32]{1,0:T(1,128)} %bitcast.15, f32[2,4096]{1,0:T(2,128)} %gain_in.1, bf16[2,32,4096]{2,1,0:T(8,128)(2,1)} %bitcast.8, bf16[2,32,4096]{2,1,0:T(8,128)(2,1)} %bitcast.9, ...), custom_call_target="tpu_custom_call" | custom-call | tf_op jit(solution)/shard_map/decode_step/pallas_call | solution.py:477
  53.3 3.4 %finish.1 = (f32[2,32,4,64,64]{4,3,2,1,0:T(8,128)}, bf16[32,256]{1,0:T(8,128)(2,1)}) custom-call(f32[2,32,4,64,64]{4,3,2,1,0:T(8,128)S(1)} %get-tuple-element.7.state_in, bf16[16,4,16,128]{3,2,1,0:T(8,128)(2,1)S(1)} %get-tuple-element.8.rows, bf16[256,4096]{1,0:T(8,128)(2,1)S(1)} %get-tuple-element.9.weight), custom_call_target="tpu_custom_call" | custom-call | tf_op jit(solution)/shard_map/finish/pallas_call | solution.py:520

commit v10 on v9

--- a/solution.py
+++ b/solution.py
@@ -13,7 +13,7 @@
 MESH = pl.DeviceIdType.MESH
 F32 = jnp.float32
 BF16 = jnp.bfloat16
-ORDERS = (("y", "x", "z"), ("z", "x", "y"), ("y", "x", "z"), ("z", "x", "y"))
+ORDERS = (("x", "y", "z"), ("x", "z", "y"), ("y", "x", "z"), ("z", "x", "y"))
 LANES = (((1,), (1,)), ((), ()))
 ROWS = (((0,), (0,)), ((), ()))
 

time: 56.8 us -> 56.8 us (level)
  no operation moved by 1% of the time
where the time goes in v10:
time: 56.8 us; the launch traced here: 56.7 us
  Pallas kernels  56 us (99%)
  between operations  0.64 us (1%)
    pallas_call x1, Pallas kernels, local(): pl.pallas_call(step_kernel, out_shape=(pltpu.VMEM(state.shape, F32), pltp...  52.6 us
    pallas_call x1, Pallas kernels, local(): pl.pallas_call(finish_kernel, out_shape=(pltpu.HBM(state.shape, F32), plt...  3.42 us

profile of v10, /device:TPU:0, one launch (start us, length us, event | category | flops | bytes accessed | tf_op | source)
XLA Modules:
  0.0 56.7 jit_solution(8385272675663402721)
XLA Ops:
  0.6 52.6 %decode_step.1 = (f32[2,32,4,64,64]{4,3,2,1,0:T(8,128)S(1)}, bf16[16,4,16,128]{3,2,1,0:T(8,128)(2,1)S(1)}, bf16[256,4096]{1,0:T(8,128)(2,1)S(1)}) custom-call(bf16[32,256]{1,0:T(8,128)(2,1)} %tok.1, s32[1,32]{1,0:T(1,128)} %bitcast.15, f32[2,4096]{1,0:T(2,128)} %gain_in.1, bf16[2,32,4096]{2,1,0:T(8,128)(2,1)} %bitcast.8, bf16[2,32,4096]{2,1,0:T(8,128)(2,1)} %bitcast.9, ...), custom_call_target="tpu_custom_call" | custom-call | tf_op jit(solution)/shard_map/decode_step/pallas_call | solution.py:477
  53.2 3.4 %finish.1 = (f32[2,32,4,64,64]{4,3,2,1,0:T(8,128)}, bf16[32,256]{1,0:T(8,128)(2,1)}) custom-call(f32[2,32,4,64,64]{4,3,2,1,0:T(8,128)S(1)} %get-tuple-element.7.state_in, bf16[16,4,16,128]{3,2,1,0:T(8,128)(2,1)S(1)} %get-tuple-element.8.rows, bf16[256,4096]{1,0:T(8,128)(2,1)S(1)} %get-tuple-element.9.weight), custom_call_target="tpu_custom_call" | custom-call | tf_op jit(solution)/shard_map/finish/pallas_call | solution.py:520
